TPU v7x, 128 devices: a whole 4x4x4 slice. The times are simulated.
128 devices in a mesh: sp: 16 (over z, y), tp: 8 (over x, core).
Axes of the slice: x: 4, y: 4, z: 4, core: 2. Of those that a mesh axis runs over, the one named last changes fastest.
Arguments:
- tokens: bfloat16 [12288, 2048], P(('sp', 'tp')), may hold values from -6 to 6
- norm_gain: float32 [2048], replicated, may hold values from 0.1 to 1.9
- w_query: bfloat16 [2048, 1024], P('sp', 'tp'), may hold values from -0.125 to 0.125
- w_forget: bfloat16 [2048, 1024], P('sp', 'tp'), may hold values from -0.125 to 0.125
- w_input: bfloat16 [2048, 1024], P('sp', 'tp'), may hold values from -0.125 to 0.125
- w_outgate: bfloat16 [2048, 1024], P('sp', 'tp'), may hold values from -0.125 to 0.125
- w_conv_value: bfloat16 [2048, 1024], P('sp', 'tp'), may hold values from -0.125 to 0.125
- w_conv_gate: bfloat16 [2048, 1024], P('sp', 'tp'), may hold values from -0.125 to 0.125
- w_gate_rec: bfloat16 [2048, 2048], P('sp', 'tp'), may hold values from -0.125 to 0.125
- w_gate_conv: bfloat16 [2048, 2048], P('sp', 'tp'), may hold values from -0.125 to 0.125
- lower_bound: float32 [1024], P('tp'), may hold values from 0.92 to 0.9999593, as said below
- decay_shift: float32 [12288, 1024], P('sp', 'tp'), may hold values from -0.7 to 0, as said below
- state_init: float32 [8, 128, 128], P('tp'), may hold values from -0.125 to 0.125
- head_gain: float32 [1024], P('tp'), may hold values from 0.1 to 1.9
- conv_kernel: float32 [31, 1024], P(None, 'tp'), may hold values from -7.5 to 7.5
- channel_gain: float32 [1024], P('tp'), may hold values from 0.1 to 1.9
- channel_bias: float32 [1024], P('tp'), may hold values from -3 to 3
- w_out_rec: bfloat16 [1024, 2048], P('tp', 'sp'), may hold values from -0.1875 to 0.1875
- w_out_conv: bfloat16 [1024, 2048], P('tp', 'sp'), may hold values from -0.1875 to 0.1875
Outputs:
- mixed_out: bfloat16 [12288, 2048], P('sp', 'tp')
Inputs may be any that keep to these rules, and one draw needn't show every extreme that they name: `lower_bound`: every entry is below one. `decay_shift`: no entry is positive.
All inputs are finite; a program needn't handle non-finite values.
Results may differ from a plain program's by a relative error of at most 0.017.
Values may be sent and summed in bfloat16 or wider, within the bound.
A program may use at most 64 MiB of HBM per device.

v0:
```python
import jax
import jax.numpy as jnp
from jax import lax
from jax.sharding import PartitionSpec as P

HEAD = 128
CONV = 1024
KW = 31
BLOCK = 64


EPSILON = 1e-06


def in_one_piece(arrays, axis, dim, along):
    ends, at = ([], 0)
    for a in arrays[:-1]:
        at += a.shape[along]
        ends.append(at)
    both = jnp.concatenate(arrays, axis=along)
    return tuple(jnp.split(lax.all_gather(both, axis, axis=dim, tiled=True), ends, axis=along))


def sent_to_all(array, axis):
    size = lax.axis_size(axis)
    return lax.all_to_all(
        jnp.broadcast_to(array[None], (size, *array.shape)), axis, 0, 0, tiled=True
    )


def all_in_one(array, axis):
    leaves = jax.tree.leaves(array)
    sequence = sorted(range(len(leaves)), key=lambda k: -leaves[k].size)
    width = (1, *leaves[sequence[0]].shape)[-1]
    lines = [
        jnp.pad(leaves[k].reshape(-1), (0, -leaves[k].size % width)).reshape(-1, width)
        for k in sequence
    ]
    both, at, found = (sent_to_all(jnp.concatenate(lines), axis), 0, {})
    for k, line in zip(sequence, lines):
        section = both[:, at : at + len(line)].reshape(len(both), -1)
        found[k] = section[:, : leaves[k].size].reshape(-1, *leaves[k].shape)
        at += len(line)
    numbers = iter(range(len(leaves)))
    return jax.tree.map(lambda _: found[next(numbers)], array)


def joined_by_halves(pieces, combine):
    while len(jax.tree.leaves(pieces)[0]) > 1:
        pieces = jax.vmap(combine)(
            *(jax.tree.map(lambda part: part[side::2], pieces) for side in (0, 1))
        )
    return jax.tree.map(lambda part: part[0], pieces)


def entering(array, axis, combine, identity):
    size, position = (lax.axis_size(axis), lax.axis_index(axis))
    passed = jnp.arange(size) < position

    def kept(part, zero, own):
        part = jnp.where(
            passed.reshape(-1, *(1 for _ in own.shape)),
            part.astype(own.dtype),
            jnp.asarray(zero, own.dtype),
        )
        return part

    pieces = all_in_one(
        jax.tree.map(lambda part, kind: part.astype(kind), array, (jnp.bfloat16, jnp.bfloat16)),
        axis,
    )
    return joined_by_halves(jax.tree.map(kept, pieces, identity, array), combine)


def passed_along(block, axis, distance):
    devices = range(lax.axis_size(axis))
    route = [(i - distance, i) for i in devices if i - distance in devices]
    return lax.ppermute(block, axis, route)


def of_everyone(array, axis):
    everything = sent_to_all(array, axis)
    return jnp.sum(everything, axis=0)


def normalize_rows(values, gain_vector):
    widened = values.astype(jnp.float32)
    scale = lax.rsqrt(jnp.mean(widened * widened, axis=-1, keepdims=True) + EPSILON)
    return (widened * scale * gain_vector).astype(jnp.bfloat16)


def block_step(state, inputs):
    query, input_gate, values, log_decay = inputs
    length = query.shape[1]
    causal_masked = (jnp.arange(length)[:, None] >= jnp.arange(length)[None, :])[None, :, :, None]
    cumulative = jnp.cumsum(log_decay, axis=1)
    spread = cumulative[:, :, None, :] - cumulative[:, None, :, :]
    weight = jnp.where(causal_masked, jnp.exp(jnp.where(causal_masked, spread, 0.0)), 0.0)
    scores = jnp.einsum("htd,hsd,htsd->hts", query, input_gate, weight)
    output = jnp.einsum("hts,hsv->htv", scores, values)
    output = output + jnp.einsum("htd,hdv->htv", query * jnp.exp(cumulative), state)
    final = cumulative[:, -1:, :]
    carried = jnp.exp(final[:, 0, :])[:, :, None] * state
    carried = carried + jnp.einsum("hsd,hsv->hdv", input_gate * jnp.exp(final - cumulative), values)
    return (carried, output)


def compose(preceding_segment, later):
    return (preceding_segment[0] * later[0], later[0][..., None] * preceding_segment[1] + later[1])


def local(
    tokens,
    norm_gain,
    w_query,
    w_forget,
    w_input,
    w_outgate,
    w_conv_value,
    w_conv_gate,
    w_gate_rec,
    w_gate_conv,
    lower_bound,
    decay_shift,
    state_init,
    head_gain,
    conv_kernel,
    channel_gain,
    channel_bias,
    w_out_rec,
    w_out_conv,
):
    tp_count = lax.axis_size("tp")
    normed = normalize_rows(lax.all_gather(tokens, "tp", axis=0, tiled=True), norm_gain)
    row_count = normed.shape[0]
    weights = (
        w_query,
        w_forget,
        w_input,
        w_outgate,
        w_conv_value,
        w_conv_gate,
        w_gate_rec,
        w_gate_conv,
    )
    portions = in_one_piece(
        (
            weights[0],
            weights[1],
            weights[2],
            weights[3],
            weights[4],
            weights[5],
            weights[6],
            weights[7],
        ),
        "sp",
        0,
        1,
    )
    sums = tuple(
        (jnp.dot(normed, portion, preferred_element_type=jnp.float32) for portion in portions)
    )
    (
        query_raw,
        forget_raw,
        input_raw,
        outgate_raw,
        value_raw,
        gate_raw,
        gate_rec_raw,
        gate_conv_raw,
    ) = tuple((overall_aggregate.astype(jnp.bfloat16) for overall_aggregate in sums))
    local_heads = w_query.shape[1] // HEAD
    block_count = row_count // BLOCK
    query = jax.nn.silu(query_raw.astype(jnp.float32))
    input_gate = (1.0 - lower_bound) * jax.nn.sigmoid(-forget_raw.astype(jnp.float32))
    log_decay = jnp.log1p(-input_gate) + decay_shift
    values = input_raw.astype(jnp.float32)

    def to_blocks(array):
        return array.reshape(block_count, BLOCK, local_heads, HEAD).transpose(0, 2, 1, 3)

    zero_state = jnp.zeros((local_heads, HEAD, HEAD), jnp.float32)
    local_state, blocks_out = lax.scan(
        block_step,
        zero_state,
        (to_blocks(query), to_blocks(input_gate), to_blocks(values), to_blocks(log_decay)),
    )
    local_out = blocks_out.transpose(0, 2, 1, 3).reshape(row_count, local_heads, HEAD)
    running = jnp.cumsum(log_decay, axis=0)
    cumulated_forgetting = jnp.exp(running[-1]).reshape(local_heads, HEAD)
    ones_decay = jnp.ones_like(cumulated_forgetting)
    prefix_decay, prefix_state = entering(
        (cumulated_forgetting, local_state), "sp", compose, (ones_decay, zero_state)
    )
    incoming_state = prefix_decay[:, :, None] * state_init + prefix_state
    decayed_query = (query * jnp.exp(running)).reshape(row_count, local_heads, HEAD)
    head_out = local_out + jnp.einsum("thd,hdv->thv", decayed_query, incoming_state)
    head_out = head_out * lax.rsqrt(jnp.mean(head_out * head_out, axis=-1, keepdims=True) + EPSILON)
    head_out = head_out * head_gain.reshape(local_heads, HEAD)
    mixed_rec = (
        head_out.reshape(row_count, local_heads * HEAD)
        * jax.nn.silu(outgate_raw.astype(jnp.float32))
    ).astype(jnp.bfloat16)
    gated = (value_raw.astype(jnp.float32) * jax.nn.sigmoid(gate_raw.astype(jnp.float32))).astype(
        jnp.bfloat16
    )
    rim_width = KW - 1
    previous = passed_along(gated[row_count - rim_width :], "sp", 1)
    extended = jnp.concatenate([previous, gated], axis=0).astype(jnp.float32)
    conv_out = jnp.zeros((row_count, gated.shape[1]), jnp.float32)
    for tap_index in range(KW):
        conv_out = conv_out + conv_kernel[tap_index] * extended[tap_index : tap_index + row_count]
    squares = of_everyone(jnp.sum(conv_out * conv_out, axis=1), "tp")
    scale = lax.rsqrt(squares / CONV + EPSILON)[:, None]
    mixed_conv = jax.nn.silu(conv_out * scale * channel_gain + channel_bias).astype(jnp.bfloat16)
    rec_columns, conv_columns = in_one_piece((w_out_rec, w_out_conv), "sp", 1, 0)
    rec_width = mixed_rec.shape[1]
    rec_whole, conv_whole = in_one_piece((rec_columns, conv_columns), "tp", 0, 1)
    both = jnp.concatenate([mixed_rec, mixed_conv], axis=1).reshape(
        tp_count, row_count // tp_count, -1
    )
    arrived = lax.all_to_all(both, "tp", split_axis=0, concat_axis=2, tiled=True)
    item_count = arrived.shape[1]
    grouped = arrived.reshape(item_count, tp_count, -1)
    rec_part = grouped[:, :, :rec_width].reshape(item_count, -1)
    conv_part = grouped[:, :, rec_width:].reshape(item_count, -1)
    first = jnp.dot(rec_part, rec_whole, preferred_element_type=jnp.float32).astype(jnp.bfloat16)
    second = jnp.dot(conv_part, conv_whole, preferred_element_type=jnp.float32).astype(jnp.bfloat16)
    projected = jnp.stack([first, second], axis=1)[None]
    returned = lax.all_to_all(projected[0], "tp", split_axis=2, concat_axis=0, tiled=True)
    y_rec = returned[:, 0]
    y_conv = returned[:, 1]
    merged = jax.nn.sigmoid(gate_rec_raw.astype(jnp.float32)) * y_rec.astype(jnp.float32)
    merged = merged + jax.nn.sigmoid(gate_conv_raw.astype(jnp.float32)) * y_conv.astype(jnp.float32)
    return merged.astype(jnp.bfloat16)


def solution(mesh):
    in_specs = (
        P(("sp", "tp"), None),
        P(),
        P("sp", "tp"),
        P("sp", "tp"),
        P("sp", "tp"),
        P("sp", "tp"),
        P("sp", "tp"),
        P("sp", "tp"),
        P("sp", "tp"),
        P("sp", "tp"),
        P("tp"),
        P("sp", "tp"),
        P("tp", None, None),
        P("tp"),
        P(None, "tp"),
        P("tp"),
        P("tp"),
        P("tp", "sp"),
        P("tp", "sp"),
    )
    out_specs = P("sp", "tp")
    return jax.shard_map(local, mesh=mesh, in_specs=in_specs, out_specs=out_specs, check_vma=False)
```

profile of v0, /device:TPU:1, one launch (start us, length us, event | category | flops | bytes accessed | tf_op | source)
XLA Modules:
  0.0 333.0 jit_solution(5961914956780123622)
XLA Ops:
  19.8 34.6 %all-gather.9.cloned.1.call-done = bf16[256,2048]{1,0:T(8,128)(2,1)} async-done(((bf16[256,128]{1,0:T(8,128)(2,1)}), bf16[256,2048]{1,0:T(8,128)(2,1)}) %all-gather.9.cloned.1.call-update) | async-done | bytes 1048592 | tf_op jit(solution)/shard_map/all_gather | solution.py:21
  56.8 28.2 %all-gather.5.cloned.1.call-done = bf16[768,2048]{1,0:T(8,128)(2,1)} async-done(((bf16[96,2048]{1,0:T(8,128)(2,1)}), bf16[768,2048]{1,0:T(8,128)(2,1)}) %all-gather.5.cloned.1.call-update) | async-done | bytes 3145744 | tf_op jit(solution)/shard_map/all_gather | solution.py:134
  85.0 2.7 fusion.28
  88.6 54.3 %all-gather.7.cloned.1.call-done = bf16[2048,1280]{1,0:T(8,128)(2,1)} async-done(((bf16[128,1280]{1,0:T(8,128)(2,1)}), bf16[2048,1280]{1,0:T(8,128)(2,1)}) %all-gather.7.cloned.1.call-update) | async-done | bytes 5242896 | tf_op jit(solution)/shard_map/all_gather | solution.py:21
  142.9 2.8 divide_multiply_fusion
  145.7 2.1 convolution_convert_fusion.6
  147.7 2.9 log-plus-one_add_fusion
  150.7 80.2 %while.13 = (s32[]{:T(128)}, f32[1,128,128]{2,1,0:T(8,128)S(1)}, f32[12,1,64,128]{3,2,1,0:T(8,128)}, f32[12,1,64,128]{3,2,1,0:T(8,128)}, f32[12,1,64,128]{3,2,1,...) while((s32[]{:T(128)}, f32[1,128,128]{2,1,0:T(8,128)S(1)}, ...), condition=%wide.region_3.4_spmd.clone, body=%wide.region_1.3_spmd.clone.sunk | while | flops 9003011 | bytes 5051520 | solution.py:185
  153.0 1.7 fusion.167
  159.7 1.7 fusion.167
  166.3 1.7 fusion.167
  173.0 1.7 fusion.167
  179.7 1.7 fusion.167
  186.4 1.7 fusion.167
  193.1 1.7 fusion.167
  219.8 1.7 fusion.167
  226.5 1.7 fusion.167
  234.1 2.2 fusion.69
  236.5 2.0 fusion.68
  238.6 3.1 collective-permute-start
  245.3 5.5 %all-to-all-start.1 = ((f32[8,1,768]{2,1,0:T(1,128)}), f32[8,1,768]{2,1,0:T(1,128)}, u32[]{:S(2)}, u32[]{:S(2)}) async-start(f32[8,1,768]{2,1,0:T(1,128)} %broadcast_in_dim.89), calls=%async_computation.1 | async-start | bytes 49152 | tf_op jit(solution)/shard_map/all_to_all | solution.py:26
  252.2 3.4 %all-to-all-done.1 = f32[8,1,768]{2,1,0:T(1,128)} async-done(((f32[8,1,768]{2,1,0:T(1,128)}), f32[8,1,768]{2,1,0:T(1,128)}, u32[]{:S(2)}, u32[]{:S(2)}) %all-to-all-start.1) | async-done | bytes 24608 | tf_op jit(solution)/shard_map/all_to_all | solution.py:26
  257.3 7.0 %all-to-all-start = ((bf16[16,129,128]{2,1,0:T(8,128)(2,1)}), bf16[16,129,128]{2,1,0:T(8,128)(2,1)}, u32[]{:S(2)}, u32[]{:S(2)}) async-start(bf16[16,129,128]{2,1,0:T(8,128)(2,1)} %broadcast_in_dim.85), calls=%async_computation | async-start | bytes 1114112 | tf_op jit(solution)/shard_map/all_to_all | solution.py:26
  266.6 8.4 %all-to-all-done = bf16[16,129,128]{2,1,0:T(8,128)(2,1)} async-done(((bf16[16,129,128]{2,1,0:T(8,128)(2,1)}), bf16[16,129,128]{2,1,0:T(8,128)(2,1)}, u32[]{:S(2)}, u32[]{:S(2)}) %all-to-all-start) | async-done | bytes 528416 | tf_op jit(solution)/shard_map/all_to_all | solution.py:26
  278.2 2.1 fusion.117
  280.3 12.6 %all_to_all.44 = bf16[8,96,256]{2,1,0:T(8,128)(2,1)S(1)} all-to-all(bf16[8,96,256]{2,1,0:T(8,128)(2,1)S(1)} %bitcast.263), channel_id=1, replica_groups=mesh['sp'=16,'tp'=8] {'tp'}, dimensions={0} | all-to-all | bytes 786432 | tf_op jit(solution)/shard_map/all_to_all | solution.py:224
  293.0 3.0 fusion.44
  296.0 3.0 fusion.41
  299.8 18.2 %all_to_all.45 = bf16[96,2,2048]{0,1,2:T(2,128)(2,1)S(1)} all-to-all(bf16[96,2,2048]{0,1,2:T(2,128)(2,1)S(1)} %copy.78), channel_id=1, replica_groups=mesh['sp'=16,'tp'=8] {'tp'}, dimensions={2} | all-to-all | bytes 1572864 | tf_op jit(solution)/shard_map/all_to_all | solution.py:232
  318.1 1.9 copy.79
  320.0 3.4 %fusion.60 = f32[768,256]{1,0:T(8,128)S(1)} fusion(bf16[768,2048]{1,0:T(8,128)(2,1)} %copy-done.1, bf16[2048,1280]{1,0:T(8,128)(2,1)} %all-gather.7.cloned.1.call-done, bf16[768,2,256]{2,0,1:T(8,128)(2,1)} %bitcast.268), kind=kOutput, calls=%fused_computation.65 | convolution fusion | flops 806682624 | bytes 5373952 | tf_op jit(solution)/shard_map/dot_general | solution.py:162
  323.5 3.0 fusion.54
  (267 shorter events, 96.8 us)
Async XLA Ops:
  6.5 47.8 %all-gather.9.cloned.1.call-start = ((), (), s32[]{:S(2)}) async-start(), calls=%async_computation.6 | async-start | bytes 1114112 | tf_op jit(solution)/shard_map/all_gather | solution.py:21
  8.0 77.0 %all-gather.5.cloned.1.call-start = ((), (), s32[]{:S(2)}) async-start(), calls=%async_computation.4 | async-start | bytes 3538944 | tf_op jit(solution)/shard_map/all_gather | solution.py:134
  8.7 134.1 %all-gather.7.cloned.1.call-start = ((), (), s32[]{:S(2)}) async-start(), calls=%async_computation.5 | async-start | bytes 5570560 | tf_op jit(solution)/shard_map/all_gather | solution.py:21
  15.8 277.2 %all-gather.11.cloned.1.call-start = ((), (), s32[]{:S(2)}) async-start(), calls=%async_computation.7 | async-start | bytes 9437184 | tf_op jit(solution)/shard_map/all_gather | solution.py:21
  55.7 32.0 %copy-start.12 = (f32[2048]{0:T(1024)S(1)}, f32[2048]{0:T(1024)}, u32[]{:S(2)}) copy-start(f32[2048]{0:T(1024)} %param.22) | copy-start | bytes 24580
  88.6 189.6 %copy-start.1 = (bf16[768,2048]{1,0:T(8,128)(2,1)}, bf16[768,2048]{1,0:T(8,128)(2,1)S(1)}, u32[]{:S(2)}) copy-start(bf16[768,2048]{1,0:T(8,128)(2,1)S(1)} %fusion.30) | copy-start | bytes 9437188
  234.1 8.2 %copy-start.4 = (f32[128,6,128]{0,2,1:T(8,128)}, f32[128,6,128]{0,2,1:T(8,128)S(1)}, u32[]{:S(2)}) copy-start(f32[128,6,128]{0,2,1:T(8,128)S(1)} %copy.72) | copy-start | bytes 1179652
  236.3 6.6 %copy-start.13 = (f32[128]{0:T(128)S(1)}, f32[128]{0:T(128)}, u32[]{:S(2)}) copy-start(f32[128]{0:T(128)} %get-tuple-element.149) | copy-start | bytes 1540
  236.3 6.6 %copy-start.14 = (f32[128]{0:T(128)S(1)}, f32[128]{0:T(128)}, u32[]{:S(2)}) copy-start(f32[128]{0:T(128)} %get-tuple-element.150) | copy-start | bytes 1540
  236.3 6.6 %copy-start.15 = (f32[128]{0:T(128)S(1)}, f32[128]{0:T(128)}, u32[]{:S(2)}) copy-start(f32[128]{0:T(128)} %get-tuple-element.151) | copy-start | bytes 1540
  236.3 6.6 %copy-start.16 = (f32[128]{0:T(128)S(1)}, f32[128]{0:T(128)}, u32[]{:S(2)}) copy-start(f32[128]{0:T(128)} %get-tuple-element.152) | copy-start | bytes 1540
  236.3 6.6 %copy-start.17 = (f32[128]{0:T(128)S(1)}, f32[128]{0:T(128)}, u32[]{:S(2)}) copy-start(f32[128]{0:T(128)} %get-tuple-element.153) | copy-start | bytes 1540
  236.3 6.6 %copy-start.18 = (f32[128]{0:T(128)S(1)}, f32[128]{0:T(128)}, u32[]{:S(2)}) copy-start(f32[128]{0:T(128)} %get-tuple-element.154) | copy-start | bytes 1540
  236.3 6.6 %copy-start.19 = (f32[128]{0:T(128)S(1)}, f32[128]{0:T(128)}, u32[]{:S(2)}) copy-start(f32[128]{0:T(128)} %get-tuple-element.155) | copy-start | bytes 1540
  236.3 6.6 %copy-start.20 = (f32[128]{0:T(128)S(1)}, f32[128]{0:T(128)}, u32[]{:S(2)}) copy-start(f32[128]{0:T(128)} %get-tuple-element.156) | copy-start | bytes 1540
  236.4 6.6 %copy-start.21 = (f32[128]{0:T(128)S(1)}, f32[128]{0:T(128)}, u32[]{:S(2)}) copy-start(f32[128]{0:T(128)} %get-tuple-element.126) | copy-start | bytes 1540
  236.4 6.6 %copy-start.22 = (f32[128]{0:T(128)S(1)}, f32[128]{0:T(128)}, u32[]{:S(2)}) copy-start(f32[128]{0:T(128)} %get-tuple-element.127) | copy-start | bytes 1540
  236.4 6.6 %copy-start.23 = (f32[128]{0:T(128)S(1)}, f32[128]{0:T(128)}, u32[]{:S(2)}) copy-start(f32[128]{0:T(128)} %get-tuple-element.128) | copy-start | bytes 1540
  236.4 6.6 %copy-start.24 = (f32[128]{0:T(128)S(1)}, f32[128]{0:T(128)}, u32[]{:S(2)}) copy-start(f32[128]{0:T(128)} %get-tuple-element.129) | copy-start | bytes 1540
  236.4 6.6 %copy-start.25 = (f32[128]{0:T(128)S(1)}, f32[128]{0:T(128)}, u32[]{:S(2)}) copy-start(f32[128]{0:T(128)} %get-tuple-element.130) | copy-start | bytes 1540
  236.4 6.6 %copy-start.26 = (f32[128]{0:T(128)S(1)}, f32[128]{0:T(128)}, u32[]{:S(2)}) copy-start(f32[128]{0:T(128)} %get-tuple-element.131) | copy-start | bytes 1540
  236.4 6.6 %copy-start.27 = (f32[128]{0:T(128)S(1)}, f32[128]{0:T(128)}, u32[]{:S(2)}) copy-start(f32[128]{0:T(128)} %get-tuple-element.132) | copy-start | bytes 1540
  236.4 6.6 %copy-start.28 = (f32[128]{0:T(128)S(1)}, f32[128]{0:T(128)}, u32[]{:S(2)}) copy-start(f32[128]{0:T(128)} %get-tuple-element.133) | copy-start | bytes 1540
  236.4 6.6 %copy-start.29 = (f32[128]{0:T(128)S(1)}, f32[128]{0:T(128)}, u32[]{:S(2)}) copy-start(f32[128]{0:T(128)} %get-tuple-element.134) | copy-start | bytes 1540
  236.4 6.6 %copy-start.30 = (f32[128]{0:T(128)S(1)}, f32[128]{0:T(128)}, u32[]{:S(2)}) copy-start(f32[128]{0:T(128)} %get-tuple-element.135) | copy-start | bytes 1540
  236.5 6.6 %copy-start.31 = (f32[128]{0:T(128)S(1)}, f32[128]{0:T(128)}, u32[]{:S(2)}) copy-start(f32[128]{0:T(128)} %get-tuple-element.136) | copy-start | bytes 1540
  236.5 6.6 %copy-start.32 = (f32[128]{0:T(128)S(1)}, f32[128]{0:T(128)}, u32[]{:S(2)}) copy-start(f32[128]{0:T(128)} %get-tuple-element.137) | copy-start | bytes 1540
  238.6 4.3 %collective-permute-start = (bf16[30,128]{1,0:T(8,128)(2,1)S(1)}, bf16[30,128]{1,0:T(8,128)(2,1)S(1)}, u32[]{:S(2)}, u32[]{:S(2)}) collective-permute-start(bf16[30,128]{1,0:T(8,128)(2,1)S(1)} %slice.369), channel_id=1, source_target_pairs={{0,8},{8,16},{16,24},{24,32},{32,40},{40,48},{48,56},{56,64},{64,7... | collective-permute-start | bytes 23048 | tf_op jit(solution)/shard_map/ppermute | solution.py:78
  245.3 10.3 %all-to-all-start.1 = ((f32[8,1,768]{2,1,0:T(1,128)}), f32[8,1,768]{2,1,0:T(1,128)}, u32[]{:S(2)}, u32[]{:S(2)}) async-start(f32[8,1,768]{2,1,0:T(1,128)} %broadcast_in_dim.89), calls=%async_computation.1 | async-start | bytes 49152 | tf_op jit(solution)/shard_map/all_to_all | solution.py:26
  257.3 17.8 %all-to-all-start = ((bf16[16,129,128]{2,1,0:T(8,128)(2,1)}), bf16[16,129,128]{2,1,0:T(8,128)(2,1)}, u32[]{:S(2)}, u32[]{:S(2)}) async-start(bf16[16,129,128]{2,1,0:T(8,128)(2,1)} %broadcast_in_dim.85), calls=%async_computation | async-start | bytes 1114112 | tf_op jit(solution)/shard_map/all_to_all | solution.py:26
  266.6 11.1 %copy-start.5 = (f32[128,6,128]{0,2,1:T(8,128)S(1)}, f32[128,6,128]{0,2,1:T(8,128)}, u32[]{:S(2)}) copy-start(f32[128,6,128]{0,2,1:T(8,128)} %copy-done.4) | copy-start | bytes 1179652
  266.6 11.5 %copy-start.41 = (f32[128]{0:T(128)S(1)}, f32[128]{0:T(128)}, u32[]{:S(2)}) copy-start(f32[128]{0:T(128)} %param.34) | copy-start | bytes 1540
  (17 other events, 69.8 us)
Sparse Core Ops, SparseCore 0:
  9.4 44.8 all-gather.8
  56.0 28.8 all-gather.4
  87.1 55.7 all-gather.6
  144.4 49.7 all-gather.10
where the time goes:
time: 338 us; the launch traced here: 333 us
  waiting for transfers between devices  130 us (38%)
  matrix products  58.7 us (17%)
  other arithmetic  47.2 us (14%)
  local copies, waits for them, and re-layouts  36.5 us (11%)
  blocking collectives  30.8 us (9%)
  starting transfers between devices  15.8 us (5%)
  between operations  13.9 us (4%)
    all_gather x3, waiting for transfers between devices, in_one_piece(): lax.all_gather(both, axis, axis=dim, tiled=True)  88.9 us
    all_gather x1, waiting for transfers between devices, local(): lax.all_gather(tokens, 'tp', axis=0, tiled=True)  28.2 us
    dot_general x12, other arithmetic, block_step(): scores = jnp.einsum('htd,hsd,htsd->hts', query, input_gate, weight)  20.5 us
    dot_general x8, matrix products, local(): jnp.dot(normed, portion, preferred_element_type=jnp.float32)  20.5 us
    all_to_all x1, blocking collectives, local(): lax.all_to_all(projected[0], 'tp', split_axis=2, concat_axis=0, tiled=True)  18.2 us
    dot_general x12, matrix products, block_step(): jnp.einsum('htd,hdv->htv', query * jnp.exp(cumulative), state)  18.2 us
    all_to_all x2, starting transfers between devices, sent_to_all(): lax.all_to_all(jnp.broadcast_to(array[None], (size, *array.shape)), axis,...  12.6 us
    all_to_all x1, blocking collectives, local(): lax.all_to_all(both, 'tp', split_axis=0, concat_axis=2, tiled=True)  12.6 us
  transfers between devices with their start and end apart: 7, of which 5 were waited for; matrix products, arithmetic and copies ran while one was open for 37% of the time, Pallas kernels for 0%

commit v1 on v0

v1 whole, which is shorter than its diff:
```python
import functools

import jax
import jax.numpy as jnp
from jax import lax
from jax.experimental import pallas as pl
from jax.experimental.pallas import tpu as pltpu
from jax.sharding import PartitionSpec as P

MESH = pl.DeviceIdType.MESH
F32 = jnp.float32
BF16 = jnp.bfloat16
HEAD = 128
CONV = 1024
KW = 31
EPS = 1e-06
L = 64
T = 768
NC = T // L
TD = 96
RT = 256
HALO = 32


class Wires:
    def __init__(self, send_sem, recv_sem):
        self.send_sem, self.recv_sem = send_sem, recv_sem
        self.count = 0
        self.sent = []

    def new(self):
        self.count += 1
        return self.count - 1

    def make(self, k, src, dst, dev):
        return pltpu.make_async_remote_copy(
            src_ref=src,
            dst_ref=dst,
            send_sem=self.send_sem.at[k],
            recv_sem=self.recv_sem.at[k],
            device_id=dev,
            device_id_type=MESH,
        )

    def start(self, k, src, dst, dev):
        copy = self.make(k, src, dst, dev)
        copy.start()
        self.sent.append(copy)

    def arrive(self, k, dst, dev):
        self.make(k, dst, dst, dev).wait_recv()


class Ring:
    def __init__(self, wires, pos, plus, minus, part, mate=None):
        self.w, self.pos, self.plus, self.minus = wires, pos, plus, minus
        self.part, self.mate = part, mate
        self.k = {n: wires.new() for n in ("L0", "L1", "R0", "R1", "F0", "F1")}
        names = ("O0", "O1", "L0", "L1", "R0", "R1", "F0", "F1")
        if mate is not None:
            self.m = {n: wires.new() for n in names}
        self.at = {
            "O": pos,
            "L": lax.rem(pos + 3, 4),
            "R": lax.rem(pos + 1, 4),
            "F": lax.rem(pos + 2, 4),
        }

    def ref(self, name):
        return self.part(self.at[name[0]], int(name[1]))

    def to_mate(self, *names):
        if self.mate is not None:
            for n in names:
                self.w.start(self.m[n], self.ref(n), self.ref(n), self.mate[0])

    def start(self):
        for n, h, dev in (
            ("L0", 0, self.plus),
            ("R1", 1, self.minus),
            ("L1", 1, self.plus),
            ("R0", 0, self.minus),
        ):
            mine = self.part(self.pos, h)
            self.w.start(self.k[n], mine, mine, dev)
        self.to_mate("O0", "O1")

    def take(self, name):
        self.w.arrive(self.k[name], self.ref(name), self.minus if name[0] == "L" else self.plus)

    def relay(self):
        self.take("L0")
        self.w.start(self.k["F0"], self.ref("L0"), self.ref("L0"), self.plus)
        self.take("R1")
        self.w.start(self.k["F1"], self.ref("R1"), self.ref("R1"), self.minus)
        self.to_mate("L0", "R1")

    def near(self):
        self.take("L1")
        self.take("R0")
        self.to_mate("L1", "R0")

    def far(self):
        self.w.arrive(self.k["F0"], self.ref("F0"), self.minus)
        self.w.arrive(self.k["F1"], self.ref("F1"), self.plus)
        self.to_mate("F0", "F1")

    def from_mate(self):
        for n in ("O0", "O1", "L0", "R1", "L1", "R0", "F0", "F1"):
            other = self.mate[1](self.at[n[0]], int(n[1]))
            self.w.arrive(self.m[n], other, self.mate[0])


def dot(a, b):
    return jnp.dot(a, b, preferred_element_type=F32)


def dot_last(a, b):
    return lax.dot_general(a, b, (((1,), (1,)), ((), ())), preferred_element_type=F32)


def dot_first(a, b):
    return lax.dot_general(a, b, (((0,), (0,)), ((), ())), preferred_element_type=F32)


def rounded(v):
    return v.astype(BF16).astype(F32)


def two(v):
    high = v.astype(BF16)
    return high, (v - high.astype(F32)).astype(BF16)


def kernel(
    tokens, gain, w_f, w_i, w_q, w_o, w_v, w_g, w_gr, w_gc, lb, shift, sinit, hgain, ck, cgain, cbias, w_or, w_oc,
    out,
    tok, gainv, xs, wb, stage, lbv, shv, siv, hgv, ckv, cgv, cbv,
    kgb, cb, vb, qb, ogb, ext, hsend, hrecv, sgr, sgc, mc, mcn, mr, head, qd, stb, rbuf, sty, stz, outv,
    load_sem, send_sem, recv_sem,
):
    s, t = lax.axis_index("sp"), lax.axis_index("tp")
    z, y, x, c = s // 4, lax.rem(s, 4), t // 2, lax.rem(t, 2)
    w = Wires(send_sem, recv_sem)

    def at(zz, yy):
        return (lax.rem(zz + 4, 4) * 4 + lax.rem(yy + 4, 4), t)

    def across(xx):
        return (s, lax.rem(xx + 4, 4) * 2 + c)

    mate = (s, 1 - c + 2 * x)
    swap = (2 * t + lax.rem(s, 2), s // 2)
    home = s // 2 == t
    following, preceding = (lax.rem(s + 1, 16), t), (lax.rem(s + 15, 16), t)

    loads = []

    def load(src, dst):
        copy = pltpu.make_async_copy(src, dst, load_sem.at[len(loads)])
        copy.start()
        loads.append(copy)
        return copy

    first = [load(tokens, tok), load(gain, gainv)]
    own = [
        load(src, wb.at[b, z, y])
        for b, src in enumerate(
            (
                w_f, w_i, w_q, w_o, w_v, w_g,
                w_gr.at[:, pl.ds(0, 128)], w_gr.at[:, pl.ds(128, 128)],
                w_gc.at[:, pl.ds(0, 128)], w_gc.at[:, pl.ds(128, 128)],
            )
        )
    ]
    staged = [load(w_or, stage.at[0]), load(w_oc, stage.at[1])]
    rest = [
        load(a, b)
        for a, b in (
            (shift, shv), (lb, lbv), (sinit.at[0], siv), (hgain, hgv), (ck, ckv), (cgain, cgv), (cbias, cbv),
        )
    ]

    barrier = pltpu.get_barrier_semaphore()
    partners = [at(z, y + 1), at(z, y - 1), at(z, y + 2), at(z + 1, y), at(z - 1, y), at(z + 2, y)]
    partners += [across(x + 1), across(x - 1), mate, following, preceding]
    for dev in partners:
        pl.semaphore_signal(barrier, inc=1, device_id=dev, device_id_type=MESH)

    @pl.when(jnp.logical_not(home))
    def _():
        pl.semaphore_signal(barrier, inc=1, device_id=swap, device_id_type=MESH)

    for copy in first:
        copy.wait()
    base = pl.multiple_of(t * TD, 16)

    def normalize(r, _):
        wide = tok[pl.ds(pl.multiple_of(r * 16, 16), 16), :].astype(F32)
        scale = lax.rsqrt(jnp.mean(wide * wide, axis=-1, keepdims=True) + EPS)
        xs[pl.ds(pl.multiple_of(base + r * 16, 16), 16), :] = (wide * scale * gainv[...]).astype(BF16)
        return 0

    lax.fori_loop(0, TD // 16, normalize, 0)
    for copy in own + staged:
        copy.wait()
    pl.semaphore_wait(barrier, len(partners) + jnp.where(home, 0, 1))

    def row_part(core):
        return lambda xx, h: xs.at[pl.ds(pl.multiple_of((xx * 2 + core) * TD + h * (TD // 2), 16), TD // 2), :]

    def half_of(buf, core):
        return lambda xx, h: buf.at[xx * 2 + core, pl.ds(384 * h, 384 if h == 0 else buf.shape[1] - 384)]

    def tp_ring(part_of):
        return Ring(w, x, across(x + 1), across(x - 1), part_of(c), (mate, part_of(1 - c)))

    token_ring = tp_ring(row_part)
    conv_ring = tp_ring(lambda core: half_of(mc, core))
    rec_ring = tp_ring(lambda core: half_of(mr, core))

    def along_y(part):
        return Ring(w, y, at(z, y + 1), at(z, y - 1), part)

    def along_z(part):
        return Ring(w, z, at(z + 1, y), at(z - 1, y), part)

    p1, p2 = [], []
    for b in range(12):
        if b % 2 == 0:
            p1.append(along_y(lambda p, h, b=b: wb.at[b, z, p, pl.ds(64 * h, 64)]))
            p2.append(along_z(lambda p, h, b=b: wb.at[b, p, pl.ds(2 * h, 2)]))
        else:
            p1.append(along_z(lambda p, h, b=b: wb.at[b, p, y, pl.ds(64 * h, 64)]))
            p2.append(along_y(lambda p, h, b=b: wb.at[b, pl.ds(2 * h, 2), p]))

    def each(rings, group, *steps):
        for step in steps:
            for b in (2 * group, 2 * group + 1):
                getattr(rings[b], step)()

    token_ring.start()
    each(p1, 0, "start")
    each(p1, 1, "start")
    swap_k = [w.new(), w.new()]

    @pl.when(jnp.logical_not(home))
    def _():
        for i in range(2):
            w.make(swap_k[i], stage.at[i], wb.at[10 + i, swap[0] // 4, lax.rem(swap[0], 4)], swap).start()

    @pl.when(home)
    def _():
        for i in range(2):
            pltpu.make_async_copy(stage.at[i], wb.at[10 + i, z, y], recv_sem.at[swap_k[i]]).start()

    each(p1, 0, "relay")
    each(p1, 1, "relay")
    each(p1, 2, "start")
    each(p1, 0, "near", "far")
    each(p2, 0, "start")
    each(p1, 2, "relay")
    each(p1, 3, "start")
    each(p1, 4, "start")
    each(p1, 1, "near", "far")
    token_ring.relay()
    each(p1, 3, "relay")
    each(p1, 4, "relay")
    each(p1, 2, "near", "far")
    each(p2, 0, "relay")
    each(p2, 1, "start")

    @pl.when(jnp.logical_not(home))
    def _():
        for i in range(2):
            w.make(swap_k[i], stage.at[i], wb.at[10 + i, z, y], swap).wait()

    @pl.when(home)
    def _():
        for i in range(2):
            pltpu.make_async_copy(stage.at[i], wb.at[10 + i, z, y], recv_sem.at[swap_k[i]]).wait()

    each(p1, 5, "start")
    token_ring.near()
    each(p1, 3, "near", "far")
    each(p1, 4, "near", "far")
    each(p1, 5, "relay")
    for copy in rest:
        copy.wait()
    each(p2, 0, "near", "far")
    each(p2, 1, "relay")
    each(p2, 2, "start")
    token_ring.far()
    token_ring.from_mate()
    each(p1, 5, "near", "far")

    def whole(b):
        return wb[b].reshape(2048, 128)

    def project(group, finish):
        weight = jnp.concatenate([whole(2 * group), whole(2 * group + 1)], axis=1)

        def tile(r, _):
            rows = pl.ds(pl.multiple_of(r * RT, RT), RT)
            finish(r, rows, dot(xs[rows, :], weight))
            return 0

        lax.fori_loop(0, T // RT, tile, 0)

    def finish_fi(r, rows, v):
        gate = (1.0 - lbv[...]) * jax.nn.sigmoid(-rounded(v[:, :128]))
        kgb[rows, :] = gate
        cb[rows, :] = jnp.log1p(-gate) + shv[rows, :]
        vb[rows, :] = v[:, 128:].astype(BF16)

    project(0, finish_fi)

    at_or_after = lax.broadcasted_iota(jnp.int32, (L, L), 0) >= lax.broadcasted_iota(jnp.int32, (L, L), 1)
    ones_below = jnp.where(at_or_after, 1.0, 0.0).astype(F32)
    state = jnp.zeros((HEAD, HEAD), F32)
    before = jnp.zeros((1, HEAD), F32)
    for i in range(NC):
        rows = pl.ds(i * L, L)
        total = jnp.dot(ones_below, cb[rows, :], precision=lax.Precision.HIGHEST, preferred_element_type=F32)
        cb[rows, :] = total
        last = total[L - 1 : L, :]
        ending = (kgb[rows, :] * jnp.exp(last - total)).astype(BF16)
        stb[i] = state.astype(BF16)
        rbuf[pl.ds(i, 1), :] = before
        state = jnp.exp(last) * state + dot_first(vb[rows, :], ending)
        before = before + last
    decay = jnp.exp(before)
    sty[y, pl.ds(0, HEAD), :] = state.astype(BF16)
    extra = jnp.concatenate([a.astype(F32) for a in two(decay)] + [jnp.zeros((14, HEAD), F32)], axis=0)
    sty[y, pl.ds(HEAD, 16), :] = extra.astype(BF16)
    y_k = [w.new() for _ in range(3)]
    z_k = [w.new() for _ in range(3)]
    for i in range(3):
        w.start(y_k[i], sty.at[y], sty.at[y], at(z, y + 1 + i))

    each(p2, 1, "near", "far")
    each(p2, 2, "relay")
    each(p2, 3, "start")

    def finish_qo(r, rows, v):
        raw = rounded(v[:, :128])
        qb[rows, :] = raw * jax.nn.sigmoid(raw)
        raw = rounded(v[:, 128:])
        ogb[rows, :] = raw * jax.nn.sigmoid(raw)

    project(1, finish_qo)

    def block_of(buf, i):
        both = buf[i, pl.ds(HEAD, 16), :].astype(F32)
        return both[0:1, :] + both[1:2, :], buf[i, pl.ds(0, HEAD), :].astype(F32)

    for i in range(3):
        w.arrive(y_k[i], sty.at[lax.rem(y + 3 - i, 4)], at(z, y + 1 + i))
    row_decay, row_state = jnp.ones((1, HEAD), F32), jnp.zeros((HEAD, HEAD), F32)
    my_decay, my_state = row_decay, row_state
    for i in range(4):
        d, v = block_of(sty, i)
        row_decay, row_state = row_decay * d, d * row_state + v
        if i < 3:
            take = i < y
            my_decay = jnp.where(take, row_decay, my_decay)
            my_state = jnp.where(take, row_state, my_state)
    stz[z, pl.ds(0, HEAD), :] = row_state.astype(BF16)
    extra = jnp.concatenate([a.astype(F32) for a in two(row_decay)] + [jnp.zeros((14, HEAD), F32)], axis=0)
    stz[z, pl.ds(HEAD, 16), :] = extra.astype(BF16)
    for i in range(3):
        w.start(z_k[i], stz.at[z], stz.at[z], at(z + 1 + i, y))

    for i in range(NC):
        rows = pl.ds(i * L, L)
        total, q = cb[rows, :], qb[rows, :]
        middle = 0.5 * total[L - 1 : L, :]
        left = (q * jnp.exp(total - middle)).astype(BF16)
        right = (kgb[rows, :] * jnp.exp(middle - total)).astype(BF16)
        scores = jnp.where(at_or_after, dot_last(left, right), 0.0).astype(BF16)
        o = dot(scores, vb[rows, :])
        o = o + dot_last((q * jnp.exp(total)).astype(BF16), stb[i])
        head[rows, :] = o
        qd[rows, :] = (q * jnp.exp(total + rbuf[pl.ds(i, 1), :])).astype(BF16)

    each(p2, 2, "near", "far")
    each(p2, 3, "relay")
    each(p2, 4, "start")

    def finish_vg(r, rows, v):
        gated = (rounded(v[:, :128]) * jax.nn.sigmoid(rounded(v[:, 128:]))).astype(BF16)
        ext[pl.ds(pl.multiple_of(r * RT + HALO, 8), RT), :] = gated.astype(F32)

    project(2, finish_vg)
    hsend[...] = ext[pl.ds(T, HALO), :].astype(BF16)
    h_k = w.new()
    w.start(h_k, hsend, hrecv, following)

    for i in range(3):
        w.arrive(z_k[i], stz.at[lax.rem(z + 3 - i, 4)], at(z + 1 + i, y))
    entering = siv[...].T
    for i in range(3):
        d, v = block_of(stz, i)
        entering = jnp.where(i < z, d * entering + v, entering)
    entering = (my_decay * entering + my_state).astype(BF16)

    def finish_head(r, _):
        rows = pl.ds(pl.multiple_of(r * RT, RT), RT)
        h = head[rows, :] + dot_last(qd[rows, :], entering)
        h = h * lax.rsqrt(jnp.mean(h * h, axis=-1, keepdims=True) + EPS) * hgv[...]
        mr[t, rows, :] = (h * ogb[rows, :]).astype(BF16)
        return 0

    lax.fori_loop(0, T // RT, finish_head, 0)
    rec_ring.start()
    each(p2, 3, "near", "far")
    each(p2, 4, "relay")
    each(p2, 5, "start")

    w.arrive(h_k, hrecv, preceding)
    ext[pl.ds(0, HALO), :] = jnp.where(s > 0, hrecv[...].astype(F32), 0.0)
    for i in range(T // 128):
        acc = jnp.zeros((128, HEAD), F32)
        for j in range(KW):
            acc = acc + ckv[pl.ds(j, 1), :] * ext[pl.ds(i * 128 + HALO - KW + 1 + j, 128), :]
        mc[t, pl.ds(i * 128, 128), :] = acc.astype(BF16)
    extra = [a.astype(F32) for v in (cgv[...], cbv[...]) for a in two(v)]
    mc[t, pl.ds(T, 16), :] = jnp.concatenate(extra + [jnp.zeros((12, HEAD), F32)], axis=0).astype(BF16)
    rec_ring.relay()
    conv_ring.start()

    def finish_gate(buf):
        def finish(r, rows, v):
            buf[rows, :] = jax.nn.sigmoid(rounded(v))

        return finish

    project(3, finish_gate(sgr))
    rec_ring.near()
    each(p2, 4, "near", "far")
    each(p2, 5, "relay")
    project(4, finish_gate(sgc))
    rec_ring.far()
    conv_ring.relay()
    each(p2, 5, "near", "far")
    rec_ring.from_mate()
    conv_ring.near()
    conv_ring.far()
    conv_ring.from_mate()

    gains, biases = [], []
    for k in range(8):
        four = mc[k, pl.ds(T, 16), :].astype(F32)
        gains.append(four[0:1, :] + four[1:2, :])
        biases.append(four[2:3, :] + four[3:4, :])

    def normalize_conv(r, _):
        rows = pl.ds(pl.multiple_of(r * 32, 32), 32)
        blocks = [mc[k, rows, :].astype(F32) for k in range(8)]
        squares = sum(v * v for v in blocks)
        scale = lax.rsqrt(jnp.sum(squares, axis=-1, keepdims=True) / CONV + EPS)
        for k in range(8):
            v = blocks[k] * scale * gains[k] + biases[k]
            mcn[rows, pl.ds(k * 128, 128)] = (v * jax.nn.sigmoid(v)).astype(BF16)
        return 0

    lax.fori_loop(0, T // 32, normalize_conv, 0)

    def out_weight(b):
        sides = [
            jnp.concatenate([wb[b, k // 2, (k % 2) * 2 + j] for k in range(8)], axis=0) for j in range(2)
        ]
        return jnp.concatenate(sides, axis=1)

    w_rec, w_conv = out_weight(10), out_weight(11)

    def last_tile(r, _):
        rows = pl.ds(pl.multiple_of(r * RT, RT), RT)
        mixed = jnp.concatenate([mr[k, rows, :] for k in range(8)], axis=1)
        merged = sgr[rows, :] * rounded(dot(mixed, w_rec))
        merged = merged + sgc[rows, :] * rounded(dot(mcn[rows, :], w_conv))
        outv[rows, :] = merged.astype(BF16)
        return 0

    lax.fori_loop(0, T // RT, last_tile, 0)
    done = pltpu.make_async_copy(outv, out, load_sem.at[0])
    done.start()
    for copy in w.sent:
        copy.wait_send()
    done.wait()


def local(
    tokens, norm_gain, w_query, w_forget, w_input, w_outgate, w_conv_value, w_conv_gate, w_gate_rec, w_gate_conv,
    lower_bound, decay_shift, state_init, head_gain, conv_kernel, channel_gain, channel_bias, w_out_rec, w_out_conv,
):
    line = lambda v: v.reshape(1, -1)
    args = (
        tokens, line(norm_gain), w_forget, w_input, w_query, w_outgate, w_conv_value, w_conv_gate, w_gate_rec,
        w_gate_conv, line(lower_bound), decay_shift, state_init, line(head_gain), conv_kernel, line(channel_gain),
        line(channel_bias), w_out_rec, w_out_conv,
    )
    v = pltpu.VMEM
    scratch = [
        v((TD, 2048), BF16), v((1, 2048), F32), v((T, 2048), BF16), v((12, 4, 4, 128, 128), BF16),
        v((2, 128, 128), BF16), v((1, 128), F32), v((T, 128), F32), v((128, 128), F32), v((1, 128), F32),
        v((KW, 128), F32), v((1, 128), F32), v((1, 128), F32),
        v((T, 128), F32), v((T, 128), F32), v((T, 128), BF16), v((T, 128), F32), v((T, 128), F32),
        v((T + HALO, 128), F32), v((HALO, 128), BF16), v((HALO, 128), BF16), v((T, 256), F32), v((T, 256), F32),
        v((8, T + 16, 128), BF16), v((T, CONV), BF16), v((8, T, 128), BF16), v((T, 128), F32), v((T, 128), BF16),
        v((NC, 128, 128), BF16), v((16, 128), F32), v((4, 144, 128), BF16), v((4, 144, 128), BF16), v((T, 256), BF16),
        pltpu.SemaphoreType.DMA((24,)), pltpu.SemaphoreType.DMA((200,)), pltpu.SemaphoreType.DMA((200,)),
    ]
    return pl.pallas_call(
        kernel,
        out_shape=jax.ShapeDtypeStruct((T, 256), BF16),
        in_specs=[pl.BlockSpec(memory_space=pl.ANY)] * len(args),
        out_specs=pl.BlockSpec(memory_space=pl.ANY),
        scratch_shapes=scratch,
        compiler_params=pltpu.CompilerParams(
            collective_id=0, has_side_effects=True, vmem_limit_bytes=56 * 1024 * 1024
        ),
    )(*args)


def solution(mesh):
    both = P("sp", "tp")
    in_specs = (
        P(("sp", "tp"), None), P(), both, both, both, both, both, both, both, both, P("tp"), both,
        P("tp", None, None), P("tp"), P(None, "tp"), P("tp"), P("tp"), P("tp", "sp"), P("tp", "sp"),
    )
    return jax.shard_map(local, mesh=mesh, in_specs=in_specs, out_specs=both, check_vma=False)
```

time: 338 us -> 75.4 us (0.22); the launches traced: 333 us -> 75.3 us
  waiting for transfers between devices: 130 us -> 0 us
  Pallas kernels: 0 us -> 73.5 us
  matrix products: 58.7 us -> 0 us
  other arithmetic: 47.2 us -> 0 us
  local copies, waits for them, and re-layouts: 36.5 us -> 1.77 us
  blocking collectives: 30.8 us -> 0 us
  starting transfers between devices: 15.8 us -> 0 us
  between operations: 13.9 us -> 0.01 us
    all_gather x4 -> x0, waiting for transfers between devices: 117 us -> none  [the longest x3 88.9 us: in_one_piece(): lax.all_gather(both, axis, axis=dim, tiled=True)]
    pallas_call x0 -> x1, Pallas kernels: none -> 73.5 us  [local(): pl.pallas_call(kernel, out_shape=jax.ShapeDtypeStruct((T, 256), BF16), in...]
    dot_general x47 -> x0, matrix products: 58.7 us -> none  [the longest x8 20.5 us: local(): jnp.dot(normed, portion, preferred_element_type=jnp.float32)]
    all_to_all x2 -> x0, blocking collectives: 30.8 us -> none  [the longest x1 18.2 us: local(): lax.all_to_all(projected[0], 'tp', split_axis=2, concat_axis=0, tiled=True)]
    dot_general x12 -> x0, other arithmetic: 20.5 us -> none  [block_step(): scores = jnp.einsum('htd,hsd,htsd->hts', query, input_gate, weight)]
    all_to_all x2 -> x0, starting transfers between devices: 12.6 us -> none  [sent_to_all(): lax.all_to_all(jnp.broadcast_to(array[None], (size, *array.shape)), axis,...]
    all_to_all x2 -> x0, waiting for transfers between devices: 11.8 us -> none  [sent_to_all(): lax.all_to_all(jnp.broadcast_to(array[None], (size, *array.shape)), axis,...]
    another operation x15 -> x0, local copies, waits for them, and re-layouts: 10.3 us -> none
  transfers between devices with their start and end apart: 7 -> 0, of which waited for: 5 -> 0; matrix products, arithmetic and copies ran while one was open for 37% -> 0% of each run, Pallas kernels for 0% -> 0%
where the time goes in v1:
time: 75.4 us; the launch traced here: 75.3 us
  Pallas kernels  73.5 us (97%)
  local copies, waits for them, and re-layouts  1.77 us (2%)
    pallas_call x1, Pallas kernels, local(): pl.pallas_call(kernel, out_shape=jax.ShapeDtypeStruct((T, 256), BF16), in...  73.5 us
    unnamed x1, local copies, waits for them, and re-layouts  1.77 us

profile of v1, /device:TPU:1, one launch (start us, length us, event | category | flops | bytes accessed | tf_op | source)
XLA Modules:
  0.0 75.3 jit_solution(14171980047023986000)
XLA Ops:
  0.0 73.5 %shard_map.181 = bf16[768,256]{1,0:T(8,128)(2,1)} custom-call(bf16[96,2048]{1,0:T(8,128)(2,1)} %tokens.1, f32[1,2048]{1,0:T(1,128)} %bitcast.5, bf16[128,128]{1,0:T(8,128)(2,1)} %w_f.1, bf16[128,128]{1,0:T(8,128)(2,1)} %w_i.1, bf16[128,128]{1,0:T(8,128)(2,1)} %w_q.1, bf16[128,128]{1,0:T(8,128)(2,1)} %w_o.1, bf16[128,128]{1,0:T(8,128)(2,1)} %w_v.1, ...), custom_call_target="tpu_custom_call" | custom-call | tf_op jit(solution)/shard_map/pallas_call | solution.py:514
  73.5 1.8 %copy.21 = bf16[768,256]{1,0:T(8,128)(2,1)} copy(bf16[768,256]{1,0:T(8,128)(2,1)} %shard_map.181) | data formatting | bytes 786432

commit v2 on v1

--- a/solution.py
+++ b/solution.py
@@ -136,7 +136,7 @@
     tokens, gain, w_f, w_i, w_q, w_o, w_v, w_g, w_gr, w_gc, lb, shift, sinit, hgain, ck, cgain, cbias, w_or, w_oc,
     out,
     tok, gainv, xs, wb, stage, lbv, shv, siv, hgv, ckv, cgv, cbv,
-    kgb, cb, vb, qb, ogb, ext, hsend, hrecv, sgr, sgc, mc, mcn, mr, head, qd, stb, rbuf, sty, stz, outv,
+    kgb, cb, vb, qb, ogb, ext, hsend, hrecv, sgr, sgc, mc, mcn, mr, head, qd, stb, rbuf, sty, stz, kv,
     load_sem, send_sem, recv_sem,
 ):
     s, t = lax.axis_index("sp"), lax.axis_index("tp")
@@ -167,7 +167,7 @@
         load(src, wb.at[b, z, y])
         for b, src in enumerate(
             (
-                w_f, w_i, w_q, w_o, w_v, w_g,
+                w_f, w_i, w_v, w_g, w_q, w_o,
                 w_gr.at[:, pl.ds(0, 128)], w_gr.at[:, pl.ds(128, 128)],
                 w_gc.at[:, pl.ds(0, 128)], w_gc.at[:, pl.ds(128, 128)],
             )
@@ -254,105 +254,152 @@
         for i in range(2):
             pltpu.make_async_copy(stage.at[i], wb.at[10 + i, z, y], recv_sem.at[swap_k[i]]).start()
 
+    def swapped():
+        @pl.when(jnp.logical_not(home))
+        def _():
+            for i in range(2):
+                w.make(swap_k[i], stage.at[i], wb.at[10 + i, z, y], swap).wait()
+
+        @pl.when(home)
+        def _():
+            for i in range(2):
+                pltpu.make_async_copy(stage.at[i], wb.at[10 + i, z, y], recv_sem.at[swap_k[i]]).wait()
+
+    def whole(b):
+        return wb[b].reshape(2048, 128)
+
+    def project(group, finish):
+        weight = jnp.concatenate([whole(2 * group), whole(2 * group + 1)], axis=1)
+
+        def tile(r, _):
+            rows = pl.ds(pl.multiple_of(r * RT, RT), RT)
+            finish(r, rows, dot(xs[rows, :], weight))
+            return 0
+
+        lax.fori_loop(0, T // RT, tile, 0)
+
+    def finish_fi(r, rows, v):
+        gate = (1.0 - lbv[...]) * jax.nn.sigmoid(-rounded(v[:, :128]))
+        kgb[rows, :] = gate
+        cb[rows, :] = jnp.log1p(-gate) + shv[rows, :]
+        vb[rows, :] = v[:, 128:].astype(BF16)
+
+    def finish_vg(r, rows, v):
+        gated = (rounded(v[:, :128]) * jax.nn.sigmoid(rounded(v[:, 128:]))).astype(BF16)
+        ext[pl.ds(pl.multiple_of(r * RT + HALO, 8), RT), :] = gated.astype(F32)
+
+    def finish_qo(r, rows, v):
+        raw = rounded(v[:, :128])
+        qb[rows, :] = raw * jax.nn.sigmoid(raw)
+        raw = rounded(v[:, 128:])
+        ogb[rows, :] = raw * jax.nn.sigmoid(raw)
+
+    def finish_gate(buf):
+        def finish(r, rows, v):
+            buf[rows, :] = jax.nn.sigmoid(rounded(v))
+
+        return finish
+
+    at_or_after = lax.broadcasted_iota(jnp.int32, (L, L), 0) >= lax.broadcasted_iota(jnp.int32, (L, L), 1)
+    ones_below = jnp.where(at_or_after, 1.0, 0.0).astype(BF16)
+
+    def pack_block(buf, i, decay, state):
+        buf[i, pl.ds(0, HEAD), :] = state.astype(BF16)
+        extra = jnp.concatenate([a.astype(F32) for a in two(decay)] + [jnp.zeros((14, HEAD), F32)], axis=0)
+        buf[i, pl.ds(HEAD, 16), :] = extra.astype(BF16)
+
+    def block_of(buf, i):
+        both = buf[i, pl.ds(HEAD, 16), :].astype(F32)
+        return both[0:1, :] + both[1:2, :], buf[i, pl.ds(0, HEAD), :].astype(F32)
+
+    def local_states():
+        for i in range(NC):
+            rows = pl.ds(i * L, L)
+            sides = dot(ones_below, jnp.concatenate(two(cb[rows, :]), axis=1))
+            total = sides[:, :128] + sides[:, 128:]
+            cb[rows, :] = total
+            ending = (kgb[rows, :] * jnp.exp(total[L - 1 : L, :] - total)).astype(BF16)
+            kv[i] = dot_first(vb[rows, :], ending)
+        state = jnp.zeros((HEAD, HEAD), F32)
+        before = jnp.zeros((1, HEAD), F32)
+        for i in range(NC):
+            last = cb[pl.ds(i * L + L - 1, 1), :]
+            stb[i] = state.astype(BF16)
+            rbuf[pl.ds(i, 1), :] = before
+            state = jnp.exp(last) * state + kv[i]
+            before = before + last
+        pack_block(sty, y, jnp.exp(before), state)
+
+    def local_outputs():
+        for i in range(NC):
+            rows = pl.ds(i * L, L)
+            total, q = cb[rows, :], qb[rows, :]
+            middle = 0.5 * total[L - 1 : L, :]
+            left = (q * jnp.exp(total - middle)).astype(BF16)
+            right = (kgb[rows, :] * jnp.exp(middle - total)).astype(BF16)
+            scores = jnp.where(at_or_after, dot_last(left, right), 0.0).astype(BF16)
+            o = dot(scores, vb[rows, :])
+            o = o + dot_last((q * jnp.exp(total)).astype(BF16), stb[i])
+            head[rows, :] = o
+            qd[rows, :] = (q * jnp.exp(total + rbuf[pl.ds(i, 1), :])).astype(BF16)
+
+    def convolve():
+        ext[pl.ds(0, HALO), :] = jnp.where(s > 0, hrecv[...].astype(F32), 0.0)
+        for i in range(T // 128):
+            acc = jnp.zeros((128, HEAD), F32)
+            for j in range(KW):
+                acc = acc + ckv[pl.ds(j, 1), :] * ext[pl.ds(i * 128 + HALO - KW + 1 + j, 128), :]
+            mc[t, pl.ds(i * 128, 128), :] = acc.astype(BF16)
+        extra = [a.astype(F32) for v in (cgv[...], cbv[...]) for a in two(v)]
+        mc[t, pl.ds(T, 16), :] = jnp.concatenate(extra + [jnp.zeros((12, HEAD), F32)], axis=0).astype(BF16)
+
+    def out_weight(b):
+        sides = [
+            jnp.concatenate([wb[b, k // 2, (k % 2) * 2 + j] for k in range(8)], axis=0) for j in range(2)
+        ]
+        return jnp.concatenate(sides, axis=1)
+
     each(p1, 0, "relay")
     each(p1, 1, "relay")
     each(p1, 2, "start")
     each(p1, 0, "near", "far")
     each(p2, 0, "start")
     each(p1, 2, "relay")
+    each(p1, 1, "near", "far")
+    each(p2, 1, "start")
+    token_ring.relay()
     each(p1, 3, "start")
+    each(p2, 0, "relay")
+    each(p1, 2, "near", "far")
+    token_ring.near()
+    each(p2, 1, "relay")
+    each(p2, 2, "start")
+    each(p1, 3, "relay")
     each(p1, 4, "start")
-    each(p1, 1, "near", "far")
-    token_ring.relay()
-    each(p1, 3, "relay")
-    each(p1, 4, "relay")
-    each(p1, 2, "near", "far")
-    each(p2, 0, "relay")
-    each(p2, 1, "start")
-
-    @pl.when(jnp.logical_not(home))
-    def _():
-        for i in range(2):
-            w.make(swap_k[i], stage.at[i], wb.at[10 + i, z, y], swap).wait()
-
-    @pl.when(home)
-    def _():
-        for i in range(2):
-            pltpu.make_async_copy(stage.at[i], wb.at[10 + i, z, y], recv_sem.at[swap_k[i]]).wait()
-
-    each(p1, 5, "start")
-    token_ring.near()
-    each(p1, 3, "near", "far")
-    each(p1, 4, "near", "far")
-    each(p1, 5, "relay")
     for copy in rest:
         copy.wait()
     each(p2, 0, "near", "far")
-    each(p2, 1, "relay")
-    each(p2, 2, "start")
     token_ring.far()
     token_ring.from_mate()
-    each(p1, 5, "near", "far")
-
-    def whole(b):
-        return wb[b].reshape(2048, 128)
-
-    def project(group, finish):
-        weight = jnp.concatenate([whole(2 * group), whole(2 * group + 1)], axis=1)
-
-        def tile(r, _):
-            rows = pl.ds(pl.multiple_of(r * RT, RT), RT)
-            finish(r, rows, dot(xs[rows, :], weight))
-            return 0
-
-        lax.fori_loop(0, T // RT, tile, 0)
-
-    def finish_fi(r, rows, v):
-        gate = (1.0 - lbv[...]) * jax.nn.sigmoid(-rounded(v[:, :128]))
-        kgb[rows, :] = gate
-        cb[rows, :] = jnp.log1p(-gate) + shv[rows, :]
-        vb[rows, :] = v[:, 128:].astype(BF16)
-
     project(0, finish_fi)
-
-    at_or_after = lax.broadcasted_iota(jnp.int32, (L, L), 0) >= lax.broadcasted_iota(jnp.int32, (L, L), 1)
-    ones_below = jnp.where(at_or_after, 1.0, 0.0).astype(F32)
-    state = jnp.zeros((HEAD, HEAD), F32)
-    before = jnp.zeros((1, HEAD), F32)
-    for i in range(NC):
-        rows = pl.ds(i * L, L)
-        total = jnp.dot(ones_below, cb[rows, :], precision=lax.Precision.HIGHEST, preferred_element_type=F32)
-        cb[rows, :] = total
-        last = total[L - 1 : L, :]
-        ending = (kgb[rows, :] * jnp.exp(last - total)).astype(BF16)
-        stb[i] = state.astype(BF16)
-        rbuf[pl.ds(i, 1), :] = before
-        state = jnp.exp(last) * state + dot_first(vb[rows, :], ending)
-        before = before + last
-    decay = jnp.exp(before)
-    sty[y, pl.ds(0, HEAD), :] = state.astype(BF16)
-    extra = jnp.concatenate([a.astype(F32) for a in two(decay)] + [jnp.zeros((14, HEAD), F32)], axis=0)
-    sty[y, pl.ds(HEAD, 16), :] = extra.astype(BF16)
+    local_states()
     y_k = [w.new() for _ in range(3)]
     z_k = [w.new() for _ in range(3)]
     for i in range(3):
         w.start(y_k[i], sty.at[y], sty.at[y], at(z, y + 1 + i))
 
+    each(p1, 3, "near", "far")
     each(p2, 1, "near", "far")
     each(p2, 2, "relay")
     each(p2, 3, "start")
-
-    def finish_qo(r, rows, v):
-        raw = rounded(v[:, :128])
-        qb[rows, :] = raw * jax.nn.sigmoid(raw)
-        raw = rounded(v[:, 128:])
-        ogb[rows, :] = raw * jax.nn.sigmoid(raw)
-
-    project(1, finish_qo)
-
-    def block_of(buf, i):
-        both = buf[i, pl.ds(HEAD, 16), :].astype(F32)
-        return both[0:1, :] + both[1:2, :], buf[i, pl.ds(0, HEAD), :].astype(F32)
+    each(p1, 4, "relay")
+    project(1, finish_vg)
+    hsend[...] = ext[pl.ds(T, HALO), :].astype(BF16)
+    h_k = w.new()
+    w.start(h_k, hsend, hrecv, following)
+    each(p1, 4, "near", "far")
+    swapped()
+    each(p1, 5, "start")
 
     for i in range(3):
         w.arrive(y_k[i], sty.at[lax.rem(y + 3 - i, 4)], at(z, y + 1 + i))
@@ -365,36 +412,20 @@
             take = i < y
             my_decay = jnp.where(take, row_decay, my_decay)
             my_state = jnp.where(take, row_state, my_state)
-    stz[z, pl.ds(0, HEAD), :] = row_state.astype(BF16)
-    extra = jnp.concatenate([a.astype(F32) for a in two(row_decay)] + [jnp.zeros((14, HEAD), F32)], axis=0)
-    stz[z, pl.ds(HEAD, 16), :] = extra.astype(BF16)
+    pack_block(stz, z, row_decay, row_state)
     for i in range(3):
         w.start(z_k[i], stz.at[z], stz.at[z], at(z + 1 + i, y))
 
-    for i in range(NC):
-        rows = pl.ds(i * L, L)
-        total, q = cb[rows, :], qb[rows, :]
-        middle = 0.5 * total[L - 1 : L, :]
-        left = (q * jnp.exp(total - middle)).astype(BF16)
-        right = (kgb[rows, :] * jnp.exp(middle - total)).astype(BF16)
-        scores = jnp.where(at_or_after, dot_last(left, right), 0.0).astype(BF16)
-        o = dot(scores, vb[rows, :])
-        o = o + dot_last((q * jnp.exp(total)).astype(BF16), stb[i])
-        head[rows, :] = o
-        qd[rows, :] = (q * jnp.exp(total + rbuf[pl.ds(i, 1), :])).astype(BF16)
-
+    w.arrive(h_k, hrecv, preceding)
+    convolve()
+    conv_ring.start()
     each(p2, 2, "near", "far")
     each(p2, 3, "relay")
     each(p2, 4, "start")
-
-    def finish_vg(r, rows, v):
-        gated = (rounded(v[:, :128]) * jax.nn.sigmoid(rounded(v[:, 128:]))).astype(BF16)
-        ext[pl.ds(pl.multiple_of(r * RT + HALO, 8), RT), :] = gated.astype(F32)
-
-    project(2, finish_vg)
-    hsend[...] = ext[pl.ds(T, HALO), :].astype(BF16)
-    h_k = w.new()
-    w.start(h_k, hsend, hrecv, following)
+    each(p1, 5, "relay")
+    project(2, finish_qo)
+    local_outputs()
+    each(p1, 5, "near", "far")
 
     for i in range(3):
         w.arrive(z_k[i], stz.at[lax.rem(z + 3 - i, 4)], at(z + 1 + i, y))
@@ -412,82 +443,59 @@
         return 0
 
     lax.fori_loop(0, T // RT, finish_head, 0)
+    conv_ring.relay()
     rec_ring.start()
     each(p2, 3, "near", "far")
     each(p2, 4, "relay")
     each(p2, 5, "start")
-
-    w.arrive(h_k, hrecv, preceding)
-    ext[pl.ds(0, HALO), :] = jnp.where(s > 0, hrecv[...].astype(F32), 0.0)
-    for i in range(T // 128):
-        acc = jnp.zeros((128, HEAD), F32)
-        for j in range(KW):
-            acc = acc + ckv[pl.ds(j, 1), :] * ext[pl.ds(i * 128 + HALO - KW + 1 + j, 128), :]
-        mc[t, pl.ds(i * 128, 128), :] = acc.astype(BF16)
-    extra = [a.astype(F32) for v in (cgv[...], cbv[...]) for a in two(v)]
-    mc[t, pl.ds(T, 16), :] = jnp.concatenate(extra + [jnp.zeros((12, HEAD), F32)], axis=0).astype(BF16)
-    rec_ring.relay()
-    conv_ring.start()
-
-    def finish_gate(buf):
-        def finish(r, rows, v):
-            buf[rows, :] = jax.nn.sigmoid(rounded(v))
-
-        return finish
-
     project(3, finish_gate(sgr))
-    rec_ring.near()
+    conv_ring.near()
     each(p2, 4, "near", "far")
     each(p2, 5, "relay")
+    rec_ring.relay()
     project(4, finish_gate(sgc))
-    rec_ring.far()
-    conv_ring.relay()
-    each(p2, 5, "near", "far")
-    rec_ring.from_mate()
-    conv_ring.near()
     conv_ring.far()
     conv_ring.from_mate()
+    rec_ring.near()
 
     gains, biases = [], []
     for k in range(8):
         four = mc[k, pl.ds(T, 16), :].astype(F32)
-        gains.append(four[0:1, :] + four[1:2, :])
-        biases.append(four[2:3, :] + four[3:4, :])
+        gains.append(0.5 * (four[0:1, :] + four[1:2, :]))
+        biases.append(0.5 * (four[2:3, :] + four[3:4, :]))
 
     def normalize_conv(r, _):
         rows = pl.ds(pl.multiple_of(r * 32, 32), 32)
         blocks = [mc[k, rows, :].astype(F32) for k in range(8)]
         squares = sum(v * v for v in blocks)
-        scale = lax.rsqrt(jnp.sum(squares, axis=-1, keepdims=True) / CONV + EPS)
+        scale = lax.rsqrt(jnp.sum(squares, axis=-1, keepdims=True) * (1.0 / CONV) + EPS)
         for k in range(8):
-            v = blocks[k] * scale * gains[k] + biases[k]
-            mcn[rows, pl.ds(k * 128, 128)] = (v * jax.nn.sigmoid(v)).astype(BF16)
+            half = blocks[k] * scale * gains[k] + biases[k]
+            mcn[rows, pl.ds(k * 128, 128)] = (half + half * jnp.tanh(half)).astype(BF16)
         return 0
 
     lax.fori_loop(0, T // 32, normalize_conv, 0)
-
-    def out_weight(b):
-        sides = [
-            jnp.concatenate([wb[b, k // 2, (k % 2) * 2 + j] for k in range(8)], axis=0) for j in range(2)
-        ]
-        return jnp.concatenate(sides, axis=1)
-
+    each(p2, 5, "near", "far")
     w_rec, w_conv = out_weight(10), out_weight(11)
+
+    def conv_tile(r, _):
+        rows = pl.ds(pl.multiple_of(r * RT, RT), RT)
+        sgc[rows, :] = sgc[rows, :] * rounded(dot(mcn[rows, :], w_conv))
+        return 0
+
+    lax.fori_loop(0, T // RT, conv_tile, 0)
+    rec_ring.far()
+    rec_ring.from_mate()
 
     def last_tile(r, _):
         rows = pl.ds(pl.multiple_of(r * RT, RT), RT)
         mixed = jnp.concatenate([mr[k, rows, :] for k in range(8)], axis=1)
-        merged = sgr[rows, :] * rounded(dot(mixed, w_rec))
-        merged = merged + sgc[rows, :] * rounded(dot(mcn[rows, :], w_conv))
-        outv[rows, :] = merged.astype(BF16)
+        out[rows, :] = (sgr[rows, :] * rounded(dot(mixed, w_rec)) + sgc[rows, :]).astype(BF16)
         return 0
 
     lax.fori_loop(0, T // RT, last_tile, 0)
-    done = pltpu.make_async_copy(outv, out, load_sem.at[0])
-    done.start()
     for copy in w.sent:
         copy.wait_send()
-    done.wait()
 
 
 def local(
@@ -508,14 +516,14 @@
         v((T, 128), F32), v((T, 128), F32), v((T, 128), BF16), v((T, 128), F32), v((T, 128), F32),
         v((T + HALO, 128), F32), v((HALO, 128), BF16), v((HALO, 128), BF16), v((T, 256), F32), v((T, 256), F32),
         v((8, T + 16, 128), BF16), v((T, CONV), BF16), v((8, T, 128), BF16), v((T, 128), F32), v((T, 128), BF16),
-        v((NC, 128, 128), BF16), v((16, 128), F32), v((4, 144, 128), BF16), v((4, 144, 128), BF16), v((T, 256), BF16),
+        v((NC, 128, 128), BF16), v((16, 128), F32), v((4, 144, 128), BF16), v((4, 144, 128), BF16), v((NC, 128, 128), F32),
         pltpu.SemaphoreType.DMA((24,)), pltpu.SemaphoreType.DMA((200,)), pltpu.SemaphoreType.DMA((200,)),
     ]
     return pl.pallas_call(
         kernel,
         out_shape=jax.ShapeDtypeStruct((T, 256), BF16),
         in_specs=[pl.BlockSpec(memory_space=pl.ANY)] * len(args),
-        out_specs=pl.BlockSpec(memory_space=pl.ANY),
+        out_specs=pl.BlockSpec(memory_space=pltpu.VMEM),
         scratch_shapes=scratch,
         compiler_params=pltpu.CompilerParams(
             collective_id=0, has_side_effects=True, vmem_limit_bytes=56 * 1024 * 1024

time: 75.4 us -> 72.9 us (0.967)
  Pallas kernels: 73.5 us -> 71 us
    pallas_call x1, Pallas kernels: 73.5 us -> 71 us  [local(): pl.pallas_call(kernel, out_shape=jax.ShapeDtypeStruct((T, 256), BF16), in...]
where the time goes in v2:
time: 72.9 us; the launch traced here: 72.8 us
  Pallas kernels  71 us (97%)
  local copies, waits for them, and re-layouts  1.77 us (2%)
    pallas_call x1, Pallas kernels, local(): pl.pallas_call(kernel, out_shape=jax.ShapeDtypeStruct((T, 256), BF16), in...  71 us
    unnamed x1, local copies, waits for them, and re-layouts  1.77 us

profile of v2, /device:TPU:1, one launch (start us, length us, event | category | flops | bytes accessed | tf_op | source)
XLA Modules:
  0.0 72.8 jit_solution(1817272024210725758)
XLA Ops:
  0.0 71.0 %shard_map.181 = bf16[768,256]{1,0:T(8,128)(2,1)} custom-call(bf16[96,2048]{1,0:T(8,128)(2,1)} %tokens.1, f32[1,2048]{1,0:T(1,128)} %bitcast.5, bf16[128,128]{1,0:T(8,128)(2,1)} %w_f.1, bf16[128,128]{1,0:T(8,128)(2,1)} %w_i.1, bf16[128,128]{1,0:T(8,128)(2,1)} %w_q.1, bf16[128,128]{1,0:T(8,128)(2,1)} %w_o.1, bf16[128,128]{1,0:T(8,128)(2,1)} %w_v.1, ...), custom_call_target="tpu_custom_call" | custom-call | tf_op jit(solution)/shard_map/pallas_call | solution.py:522
  71.0 1.8 %copy.21 = bf16[768,256]{1,0:T(8,128)(2,1)} copy(bf16[768,256]{1,0:T(8,128)(2,1)} %shard_map.181) | data formatting | bytes 786432

commit v3 on v2

--- a/solution.py
+++ b/solution.py
@@ -19,6 +19,8 @@
 NC = T // L
 TD = 96
 RT = 256
+XT = 192
+PT = 384
 HALO = 32
 
 
@@ -105,8 +107,14 @@
         self.w.arrive(self.k["F1"], self.ref("F1"), self.plus)
         self.to_mate("F0", "F1")
 
-    def from_mate(self):
-        for n in ("O0", "O1", "L0", "R1", "L1", "R0", "F0", "F1"):
+    def mate_near(self):
+        self.from_mate("O0", "O1", "L0", "R1", "L1", "R0")
+
+    def mate_far(self):
+        self.from_mate("F0", "F1")
+
+    def from_mate(self, *names):
+        for n in names:
             other = self.mate[1](self.at[n[0]], int(n[1]))
             self.w.arrive(self.m[n], other, self.mate[0])
 
@@ -136,7 +144,7 @@
     tokens, gain, w_f, w_i, w_q, w_o, w_v, w_g, w_gr, w_gc, lb, shift, sinit, hgain, ck, cgain, cbias, w_or, w_oc,
     out,
     tok, gainv, xs, wb, stage, lbv, shv, siv, hgv, ckv, cgv, cbv,
-    kgb, cb, vb, qb, ogb, ext, hsend, hrecv, sgr, sgc, mc, mcn, mr, head, qd, stb, rbuf, sty, stz, kv,
+    kgb, cb, vb, qb, ogb, ext, hsend, hrecv, sgr, sgc, mc, mcn, mr, head, qd, stb, rbuf, sty, stz, kv, scales,
     load_sem, send_sem, recv_sem,
 ):
     s, t = lax.axis_index("sp"), lax.axis_index("tp")
@@ -167,7 +175,7 @@
         load(src, wb.at[b, z, y])
         for b, src in enumerate(
             (
-                w_f, w_i, w_v, w_g, w_q, w_o,
+                w_v, w_g, w_f, w_i, w_q, w_o,
                 w_gr.at[:, pl.ds(0, 128)], w_gr.at[:, pl.ds(128, 128)],
                 w_gc.at[:, pl.ds(0, 128)], w_gc.at[:, pl.ds(128, 128)],
             )
@@ -239,9 +247,9 @@
             for b in (2 * group, 2 * group + 1):
                 getattr(rings[b], step)()
 
-    token_ring.start()
     each(p1, 0, "start")
     each(p1, 1, "start")
+    token_ring.start()
     swap_k = [w.new(), w.new()]
 
     @pl.when(jnp.logical_not(home))
@@ -268,34 +276,41 @@
     def whole(b):
         return wb[b].reshape(2048, 128)
 
-    def project(group, finish):
+    def project(group, finish, size, starts):
         weight = jnp.concatenate([whole(2 * group), whole(2 * group + 1)], axis=1)
 
         def tile(r, _):
-            rows = pl.ds(pl.multiple_of(r * RT, RT), RT)
-            finish(r, rows, dot(xs[rows, :], weight))
+            start = pl.multiple_of(starts(r), 32)
+            rows = pl.ds(start, size)
+            finish(start, rows, dot(xs[rows, :], weight))
             return 0
 
-        lax.fori_loop(0, T // RT, tile, 0)
-
-    def finish_fi(r, rows, v):
+        return lambda low, high: lax.fori_loop(low, high, tile, 0)
+
+    def project_all(group, finish):
+        project(group, finish, PT, lambda r: r * PT)(0, T // PT)
+
+    def by_ring(r):
+        return lax.rem(x + jnp.where(r == 1, 3, jnp.where(r == 2, 1, jnp.where(r == 3, 2, 0))), 4) * XT
+
+    def finish_fi(start, rows, v):
         gate = (1.0 - lbv[...]) * jax.nn.sigmoid(-rounded(v[:, :128]))
         kgb[rows, :] = gate
         cb[rows, :] = jnp.log1p(-gate) + shv[rows, :]
         vb[rows, :] = v[:, 128:].astype(BF16)
 
-    def finish_vg(r, rows, v):
+    def finish_vg(start, rows, v):
         gated = (rounded(v[:, :128]) * jax.nn.sigmoid(rounded(v[:, 128:]))).astype(BF16)
-        ext[pl.ds(pl.multiple_of(r * RT + HALO, 8), RT), :] = gated.astype(F32)
-
-    def finish_qo(r, rows, v):
+        ext[pl.ds(pl.multiple_of(start + HALO, 8), XT), :] = gated.astype(F32)
+
+    def finish_qo(start, rows, v):
         raw = rounded(v[:, :128])
         qb[rows, :] = raw * jax.nn.sigmoid(raw)
         raw = rounded(v[:, 128:])
         ogb[rows, :] = raw * jax.nn.sigmoid(raw)
 
     def finish_gate(buf):
-        def finish(r, rows, v):
+        def finish(start, rows, v):
             buf[rows, :] = jax.nn.sigmoid(rounded(v))
 
         return finish
@@ -364,42 +379,47 @@
     each(p1, 2, "start")
     each(p1, 0, "near", "far")
     each(p2, 0, "start")
-    each(p1, 2, "relay")
     each(p1, 1, "near", "far")
     each(p2, 1, "start")
+    each(p1, 2, "relay")
     token_ring.relay()
-    each(p1, 3, "start")
     each(p2, 0, "relay")
     each(p1, 2, "near", "far")
     token_ring.near()
     each(p2, 1, "relay")
     each(p2, 2, "start")
-    each(p1, 3, "relay")
-    each(p1, 4, "start")
     for copy in rest:
         copy.wait()
     each(p2, 0, "near", "far")
+    token_ring.mate_near()
+    project_vg = project(0, finish_vg, XT, by_ring)
+    project_vg(0, 3)
+    each(p1, 3, "start")
     token_ring.far()
-    token_ring.from_mate()
-    project(0, finish_fi)
+    each(p2, 2, "relay")
+    each(p1, 4, "start")
+    token_ring.mate_far()
+    project_vg(3, 4)
+    hsend[...] = ext[pl.ds(T, HALO), :].astype(BF16)
+    h_k = w.new()
+    w.start(h_k, hsend, hrecv, following)
+    each(p2, 1, "near", "far")
+    project_all(1, finish_fi)
     local_states()
     y_k = [w.new() for _ in range(3)]
     z_k = [w.new() for _ in range(3)]
     for i in range(3):
         w.start(y_k[i], sty.at[y], sty.at[y], at(z, y + 1 + i))
 
+    each(p1, 3, "relay")
+    each(p1, 4, "relay")
+    w.arrive(h_k, hrecv, preceding)
+    convolve()
+    conv_ring.start()
     each(p1, 3, "near", "far")
-    each(p2, 1, "near", "far")
-    each(p2, 2, "relay")
     each(p2, 3, "start")
-    each(p1, 4, "relay")
-    project(1, finish_vg)
-    hsend[...] = ext[pl.ds(T, HALO), :].astype(BF16)
-    h_k = w.new()
-    w.start(h_k, hsend, hrecv, following)
-    each(p1, 4, "near", "far")
-    swapped()
-    each(p1, 5, "start")
+    each(p2, 2, "near", "far")
+    project_all(2, finish_qo)
 
     for i in range(3):
         w.arrive(y_k[i], sty.at[lax.rem(y + 3 - i, 4)], at(z, y + 1 + i))
@@ -416,16 +436,13 @@
     for i in range(3):
         w.start(z_k[i], stz.at[z], stz.at[z], at(z + 1 + i, y))
 
-    w.arrive(h_k, hrecv, preceding)
-    convolve()
-    conv_ring.start()
-    each(p2, 2, "near", "far")
+    each(p1, 4, "near", "far")
+    local_outputs()
     each(p2, 3, "relay")
     each(p2, 4, "start")
-    each(p1, 5, "relay")
-    project(2, finish_qo)
-    local_outputs()
-    each(p1, 5, "near", "far")
+    swapped()
+    each(p1, 5, "start")
+    conv_ring.relay()
 
     for i in range(3):
         w.arrive(z_k[i], stz.at[lax.rem(z + 3 - i, 4)], at(z + 1 + i, y))
@@ -443,20 +460,18 @@
         return 0
 
     lax.fori_loop(0, T // RT, finish_head, 0)
-    conv_ring.relay()
     rec_ring.start()
+    each(p1, 5, "relay")
+    each(p2, 4, "relay")
+    conv_ring.near()
     each(p2, 3, "near", "far")
-    each(p2, 4, "relay")
+    project_all(3, finish_gate(sgr))
+    each(p1, 5, "near", "far")
     each(p2, 5, "start")
-    project(3, finish_gate(sgr))
-    conv_ring.near()
-    each(p2, 4, "near", "far")
-    each(p2, 5, "relay")
+    conv_ring.far()
     rec_ring.relay()
-    project(4, finish_gate(sgc))
-    conv_ring.far()
-    conv_ring.from_mate()
-    rec_ring.near()
+    conv_ring.mate_near()
+    conv_ring.mate_far()
 
     gains, biases = [], []
     for k in range(8):
@@ -464,17 +479,27 @@
         gains.append(0.5 * (four[0:1, :] + four[1:2, :]))
         biases.append(0.5 * (four[2:3, :] + four[3:4, :]))
 
+    def conv_scale(r, _):
+        rows = pl.ds(pl.multiple_of(r * 64, 64), 64)
+        squares = sum(v * v for v in (mc[k, rows, :].astype(F32) for k in range(8)))
+        scale = lax.rsqrt(jnp.sum(squares, axis=-1, keepdims=True) * (1.0 / CONV) + EPS)
+        scales[rows, :] = jnp.broadcast_to(scale, (64, 128))
+        return 0
+
     def normalize_conv(r, _):
-        rows = pl.ds(pl.multiple_of(r * 32, 32), 32)
-        blocks = [mc[k, rows, :].astype(F32) for k in range(8)]
-        squares = sum(v * v for v in blocks)
-        scale = lax.rsqrt(jnp.sum(squares, axis=-1, keepdims=True) * (1.0 / CONV) + EPS)
+        rows = pl.ds(pl.multiple_of(r * 64, 64), 64)
+        scale = scales[rows, :]
         for k in range(8):
-            half = blocks[k] * scale * gains[k] + biases[k]
+            half = mc[k, rows, :].astype(F32) * scale * gains[k] + biases[k]
             mcn[rows, pl.ds(k * 128, 128)] = (half + half * jnp.tanh(half)).astype(BF16)
         return 0
 
-    lax.fori_loop(0, T // 32, normalize_conv, 0)
+    lax.fori_loop(0, T // 64, conv_scale, 0, unroll=4)
+    lax.fori_loop(0, T // 64, normalize_conv, 0, unroll=2)
+    each(p2, 5, "relay")
+    rec_ring.near()
+    each(p2, 4, "near", "far")
+    project_all(4, finish_gate(sgc))
     each(p2, 5, "near", "far")
     w_rec, w_conv = out_weight(10), out_weight(11)
 
@@ -485,7 +510,8 @@
 
     lax.fori_loop(0, T // RT, conv_tile, 0)
     rec_ring.far()
-    rec_ring.from_mate()
+    rec_ring.mate_near()
+    rec_ring.mate_far()
 
     def last_tile(r, _):
         rows = pl.ds(pl.multiple_of(r * RT, RT), RT)
@@ -516,13 +542,13 @@
         v((T, 128), F32), v((T, 128), F32), v((T, 128), BF16), v((T, 128), F32), v((T, 128), F32),
         v((T + HALO, 128), F32), v((HALO, 128), BF16), v((HALO, 128), BF16), v((T, 256), F32), v((T, 256), F32),
         v((8, T + 16, 128), BF16), v((T, CONV), BF16), v((8, T, 128), BF16), v((T, 128), F32), v((T, 128), BF16),
-        v((NC, 128, 128), BF16), v((16, 128), F32), v((4, 144, 128), BF16), v((4, 144, 128), BF16), v((NC, 128, 128), F32),
+        v((NC, 128, 128), BF16), v((16, 128), F32), v((4, 144, 128), BF16), v((4, 144, 128), BF16), v((NC, 128, 128), F32), v((T, 128), F32),
         pltpu.SemaphoreType.DMA((24,)), pltpu.SemaphoreType.DMA((200,)), pltpu.SemaphoreType.DMA((200,)),
     ]
     return pl.pallas_call(
         kernel,
         out_shape=jax.ShapeDtypeStruct((T, 256), BF16),
-        in_specs=[pl.BlockSpec(memory_space=pl.ANY)] * len(args),
+        in_specs=[pl.BlockSpec(memory_space=pltpu.HBM)] * len(args),
         out_specs=pl.BlockSpec(memory_space=pltpu.VMEM),
         scratch_shapes=scratch,
         compiler_params=pltpu.CompilerParams(

time: 72.9 us -> 67.1 us (0.920)
  Pallas kernels: 71 us -> 65.2 us
    pallas_call x1, Pallas kernels: 71 us -> 65.2 us  [local(): pl.pallas_call(kernel, out_shape=jax.ShapeDtypeStruct((T, 256), BF16), in...]
where the time goes in v3:
time: 67.1 us; the launch traced here: 66.9 us
  Pallas kernels  65.2 us (97%)
  local copies, waits for them, and re-layouts  1.77 us (3%)
    pallas_call x1, Pallas kernels, local(): pl.pallas_call(kernel, out_shape=jax.ShapeDtypeStruct((T, 256), BF16), in...  65.2 us
    unnamed x1, local copies, waits for them, and re-layouts  1.77 us

profile of v3, /device:TPU:1, one launch (start us, length us, event | category | flops | bytes accessed | tf_op | source)
XLA Modules:
  0.0 66.9 jit_solution(3646908285870655116)
XLA Ops:
  0.0 65.2 %shard_map.181 = bf16[768,256]{1,0:T(8,128)(2,1)} custom-call(bf16[96,2048]{1,0:T(8,128)(2,1)} %tokens.1, f32[1,2048]{1,0:T(1,128)} %bitcast.5, bf16[128,128]{1,0:T(8,128)(2,1)} %w_f.1, bf16[128,128]{1,0:T(8,128)(2,1)} %w_i.1, bf16[128,128]{1,0:T(8,128)(2,1)} %w_q.1, bf16[128,128]{1,0:T(8,128)(2,1)} %w_o.1, bf16[128,128]{1,0:T(8,128)(2,1)} %w_v.1, ...), custom_call_target="tpu_custom_call" | custom-call | tf_op jit(solution)/shard_map/pallas_call | solution.py:548
  65.2 1.8 %copy.21 = bf16[768,256]{1,0:T(8,128)(2,1)} copy(bf16[768,256]{1,0:T(8,128)(2,1)} %shard_map.181) | data formatting | bytes 786432

commit v4 on v3

--- a/solution.py
+++ b/solution.py
@@ -28,95 +28,91 @@
     def __init__(self, send_sem, recv_sem):
         self.send_sem, self.recv_sem = send_sem, recv_sem
         self.count = 0
-        self.sent = []
 
     def new(self):
         self.count += 1
         return self.count - 1
 
-    def make(self, k, src, dst, dev):
+    def make(self, lane, k, src, dst, dev):
         return pltpu.make_async_remote_copy(
             src_ref=src,
             dst_ref=dst,
-            send_sem=self.send_sem.at[k],
+            send_sem=self.send_sem.at[lane],
             recv_sem=self.recv_sem.at[k],
             device_id=dev,
             device_id_type=MESH,
         )
 
-    def start(self, k, src, dst, dev):
-        copy = self.make(k, src, dst, dev)
-        copy.start()
-        self.sent.append(copy)
-
-    def arrive(self, k, dst, dev):
-        self.make(k, dst, dst, dev).wait_recv()
-
-
-class Ring:
-    def __init__(self, wires, pos, plus, minus, part, mate=None):
-        self.w, self.pos, self.plus, self.minus = wires, pos, plus, minus
-        self.part, self.mate = part, mate
-        self.k = {n: wires.new() for n in ("L0", "L1", "R0", "R1", "F0", "F1")}
-        names = ("O0", "O1", "L0", "L1", "R0", "R1", "F0", "F1")
+    def start(self, lane, k, src, dst, dev):
+        self.make(lane, k, src, dst, dev).start()
+
+    def arrive(self, k, span, dev):
+        self.make(0, k, span, span, dev).wait_recv()
+
+    def left(self, lane, span, dev):
+        self.make(lane, 0, span, span, dev).wait_send()
+
+
+class Exchange:
+    def __init__(self, wires, lane, rings, span, mate=None):
+        self.w, self.lane, self.rings, self.span, self.mate = wires, lane, rings, span, mate
+        self.k = {"relay": wires.new(), "near": wires.new()}
+        self.k["far"] = self.k["near"] if mate is None else wires.new()
         if mate is not None:
-            self.m = {n: wires.new() for n in names}
-        self.at = {
-            "O": pos,
-            "L": lax.rem(pos + 3, 4),
-            "R": lax.rem(pos + 1, 4),
-            "F": lax.rem(pos + 2, 4),
-        }
-
-    def ref(self, name):
-        return self.part(self.at[name[0]], int(name[1]))
-
-    def to_mate(self, *names):
+            self.k["mate_near"], self.k["mate_far"] = wires.new(), wires.new()
+
+    def go(self, sem, view, dev):
+        self.w.start(self.lane, self.k[sem], view, view, dev)
+
+    def to_mate(self, sem, *views):
         if self.mate is not None:
-            for n in names:
-                self.w.start(self.m[n], self.ref(n), self.ref(n), self.mate[0])
+            for view in views:
+                self.go(sem, view, self.mate)
+
+    def await_blocks(self, sem, n):
+        self.w.arrive(self.k[sem], self.span(n * len(self.rings)), self.rings[0][1])
+
+    def first(self):
+        for pos, plus, minus, part in self.rings:
+            self.go("relay", part(pos, 0), plus)
+            self.go("relay", part(pos, 1), minus)
+
+    def second(self):
+        for pos, plus, minus, part in self.rings:
+            self.go("near", part(pos, 1), plus)
+            self.go("near", part(pos, 0), minus)
+            self.to_mate("mate_near", part(pos, 0), part(pos, 1))
 
     def start(self):
-        for n, h, dev in (
-            ("L0", 0, self.plus),
-            ("R1", 1, self.minus),
-            ("L1", 1, self.plus),
-            ("R0", 0, self.minus),
-        ):
-            mine = self.part(self.pos, h)
-            self.w.start(self.k[n], mine, mine, dev)
-        self.to_mate("O0", "O1")
-
-    def take(self, name):
-        self.w.arrive(self.k[name], self.ref(name), self.minus if name[0] == "L" else self.plus)
+        self.first()
+        self.second()
 
     def relay(self):
-        self.take("L0")
-        self.w.start(self.k["F0"], self.ref("L0"), self.ref("L0"), self.plus)
-        self.take("R1")
-        self.w.start(self.k["F1"], self.ref("R1"), self.ref("R1"), self.minus)
-        self.to_mate("L0", "R1")
+        self.await_blocks("relay", 1)
+        for pos, plus, minus, part in self.rings:
+            left, right = part(lax.rem(pos + 3, 4), 0), part(lax.rem(pos + 1, 4), 1)
+            self.go("far", left, plus)
+            self.go("far", right, minus)
+            self.to_mate("mate_near", left, right)
 
     def near(self):
-        self.take("L1")
-        self.take("R0")
-        self.to_mate("L1", "R0")
+        self.await_blocks("near", 1)
+        for pos, plus, minus, part in self.rings:
+            self.to_mate("mate_near", part(lax.rem(pos + 3, 4), 1), part(lax.rem(pos + 1, 4), 0))
 
     def far(self):
-        self.w.arrive(self.k["F0"], self.ref("F0"), self.minus)
-        self.w.arrive(self.k["F1"], self.ref("F1"), self.plus)
-        self.to_mate("F0", "F1")
+        self.await_blocks("far", 1)
+        for pos, plus, minus, part in self.rings:
+            self.to_mate("mate_far", part(lax.rem(pos + 2, 4), 0), part(lax.rem(pos + 2, 4), 1))
+
+    def rest(self):
+        self.await_blocks("near", 2)
 
     def mate_near(self):
-        self.from_mate("O0", "O1", "L0", "R1", "L1", "R0")
+        self.w.arrive(self.k["mate_near"], self.span(3), self.mate)
 
     def mate_far(self):
-        self.from_mate("F0", "F1")
-
-    def from_mate(self, *names):
-        for n in names:
-            other = self.mate[1](self.at[n[0]], int(n[1]))
-            self.w.arrive(self.m[n], other, self.mate[0])
+        self.w.arrive(self.k["mate_far"], self.span(1), self.mate)
 
 
 def dot(a, b):
@@ -162,30 +158,30 @@
     home = s // 2 == t
     following, preceding = (lax.rem(s + 1, 16), t), (lax.rem(s + 15, 16), t)
 
-    loads = []
-
-    def load(src, dst):
-        copy = pltpu.make_async_copy(src, dst, load_sem.at[len(loads)])
+    def load(k, src, dst):
+        copy = pltpu.make_async_copy(src, dst, load_sem.at[k])
         copy.start()
-        loads.append(copy)
         return copy
 
-    first = [load(tokens, tok), load(gain, gainv)]
-    own = [
-        load(src, wb.at[b, z, y])
-        for b, src in enumerate(
+    first = [load(0, tokens, tok), load(1, gain, gainv)]
+    for b, src in enumerate(
+        (
+            w_v, w_g, w_f, w_i, w_q, w_o,
+            w_gr.at[:, pl.ds(0, 128)], w_gr.at[:, pl.ds(128, 128)],
+            w_gc.at[:, pl.ds(0, 128)], w_gc.at[:, pl.ds(128, 128)],
+        )
+    ):
+        load(2, src, wb.at[b, z, y])
+    load(2, w_or, stage.at[0])
+    load(2, w_oc, stage.at[1])
+    twelve = wb.at[0, pl.ds(0, 3)]
+    own = pltpu.make_async_copy(twelve, twelve, load_sem.at[2])
+    rest = [
+        load(k + 3, a, b)
+        for k, (a, b) in enumerate(
             (
-                w_v, w_g, w_f, w_i, w_q, w_o,
-                w_gr.at[:, pl.ds(0, 128)], w_gr.at[:, pl.ds(128, 128)],
-                w_gc.at[:, pl.ds(0, 128)], w_gc.at[:, pl.ds(128, 128)],
+                (shift, shv), (lb, lbv), (sinit.at[0], siv), (hgain, hgv), (ck, ckv), (cgain, cgv), (cbias, cbv),
             )
-        )
-    ]
-    staged = [load(w_or, stage.at[0]), load(w_oc, stage.at[1])]
-    rest = [
-        load(a, b)
-        for a, b in (
-            (shift, shv), (lb, lbv), (sinit.at[0], siv), (hgain, hgv), (ck, ckv), (cgain, cgv), (cbias, cbv),
         )
     ]
 
@@ -210,8 +206,7 @@
         return 0
 
     lax.fori_loop(0, TD // 16, normalize, 0)
-    for copy in own + staged:
-        copy.wait()
+    own.wait()
     pl.semaphore_wait(barrier, len(partners) + jnp.where(home, 0, 1))
 
     def row_part(core):
@@ -220,58 +215,60 @@
     def half_of(buf, core):
         return lambda xx, h: buf.at[xx * 2 + core, pl.ds(384 * h, 384 if h == 0 else buf.shape[1] - 384)]
 
-    def tp_ring(part_of):
-        return Ring(w, x, across(x + 1), across(x - 1), part_of(c), (mate, part_of(1 - c)))
-
-    token_ring = tp_ring(row_part)
-    conv_ring = tp_ring(lambda core: half_of(mc, core))
-    rec_ring = tp_ring(lambda core: half_of(mr, core))
+    def tp_exchange(lane, part, span):
+        return Exchange(w, lane, [(x, across(x + 1), across(x - 1), part)], span, mate)
+
+    token_ring = tp_exchange(1, row_part(c), lambda n: xs.at[pl.ds(0, TD * n), :])
+    conv_ring = tp_exchange(2, half_of(mc, c), lambda n: mc.at[pl.ds(0, n)])
+    rec_ring = tp_exchange(3, half_of(mr, c), lambda n: mr.at[pl.ds(0, n)])
 
     def along_y(part):
-        return Ring(w, y, at(z, y + 1), at(z, y - 1), part)
+        return (y, at(z, y + 1), at(z, y - 1), part)
 
     def along_z(part):
-        return Ring(w, z, at(z + 1, y), at(z - 1, y), part)
+        return (z, at(z + 1, y), at(z - 1, y), part)
 
     p1, p2 = [], []
-    for b in range(12):
-        if b % 2 == 0:
-            p1.append(along_y(lambda p, h, b=b: wb.at[b, z, p, pl.ds(64 * h, 64)]))
-            p2.append(along_z(lambda p, h, b=b: wb.at[b, p, pl.ds(2 * h, 2)]))
-        else:
-            p1.append(along_z(lambda p, h, b=b: wb.at[b, p, y, pl.ds(64 * h, 64)]))
-            p2.append(along_y(lambda p, h, b=b: wb.at[b, pl.ds(2 * h, 2), p]))
-
-    def each(rings, group, *steps):
-        for step in steps:
-            for b in (2 * group, 2 * group + 1):
-                getattr(rings[b], step)()
-
-    each(p1, 0, "start")
-    each(p1, 1, "start")
+    for g in range(6):
+        a, b = 2 * g, 2 * g + 1
+        rings = [
+            along_y(lambda p, h, b=a: wb.at[b, z, p, pl.ds(64 * h, 64)]),
+            along_z(lambda p, h, b=b: wb.at[b, p, y, pl.ds(64 * h, 64)]),
+        ]
+        p1.append(Exchange(w, 0, rings, lambda n, b=a: wb.at[b, 0, pl.ds(0, n)]))
+        rings = [
+            along_z(lambda p, h, b=a: wb.at[b, p, pl.ds(2 * h, 2)]),
+            along_y(lambda p, h, b=b: wb.at[b, pl.ds(2 * h, 2), p]),
+        ]
+        p2.append(Exchange(w, 8, rings, lambda n, b=a: wb.at[b, pl.ds(0, n)]))
+
+    for g in range(5):
+        p1[g].start()
     token_ring.start()
-    swap_k = [w.new(), w.new()]
+    swap_k = w.new()
+
+    def place(i):
+        return wb.at[10 + i, swap[0] // 4, lax.rem(swap[0], 4)]
 
     @pl.when(jnp.logical_not(home))
     def _():
         for i in range(2):
-            w.make(swap_k[i], stage.at[i], wb.at[10 + i, swap[0] // 4, lax.rem(swap[0], 4)], swap).start()
+            w.start(4, swap_k, stage.at[i], place(i), swap)
 
     @pl.when(home)
     def _():
         for i in range(2):
-            pltpu.make_async_copy(stage.at[i], wb.at[10 + i, z, y], recv_sem.at[swap_k[i]]).start()
+            pltpu.make_async_copy(stage.at[i], wb.at[10 + i, z, y], recv_sem.at[swap_k]).start()
 
     def swapped():
         @pl.when(jnp.logical_not(home))
         def _():
-            for i in range(2):
-                w.make(swap_k[i], stage.at[i], wb.at[10 + i, z, y], swap).wait()
+            w.arrive(swap_k, stage, swap)
+            w.left(4, stage, swap)
 
         @pl.when(home)
         def _():
-            for i in range(2):
-                pltpu.make_async_copy(stage.at[i], wb.at[10 + i, z, y], recv_sem.at[swap_k[i]]).wait()
+            pltpu.make_async_copy(stage, stage, recv_sem.at[swap_k]).wait()
 
     def whole(b):
         return wb[b].reshape(2048, 128)
@@ -374,55 +371,60 @@
         ]
         return jnp.concatenate(sides, axis=1)
 
-    each(p1, 0, "relay")
-    each(p1, 1, "relay")
-    each(p1, 2, "start")
-    each(p1, 0, "near", "far")
-    each(p2, 0, "start")
-    each(p1, 1, "near", "far")
-    each(p2, 1, "start")
-    each(p1, 2, "relay")
+    p1[0].relay()
+    p1[1].relay()
+    p1[2].relay()
+    p1[3].relay()
+    p1[4].relay()
+    p1[0].rest()
+    p2[0].first()
+    p2[0].second()
+    p1[1].rest()
+    p2[1].first()
     token_ring.relay()
-    each(p2, 0, "relay")
-    each(p1, 2, "near", "far")
+    p1[2].rest()
+    p1[3].rest()
+    p1[4].rest()
+    p2[0].relay()
+    p2[1].second()
     token_ring.near()
-    each(p2, 1, "relay")
-    each(p2, 2, "start")
+    p2[1].relay()
+    p2[2].first()
     for copy in rest:
         copy.wait()
-    each(p2, 0, "near", "far")
+    p2[0].rest()
     token_ring.mate_near()
     project_vg = project(0, finish_vg, XT, by_ring)
     project_vg(0, 3)
-    each(p1, 3, "start")
+    p2[2].second()
+    swapped()
+    p1[5].start()
     token_ring.far()
-    each(p2, 2, "relay")
-    each(p1, 4, "start")
     token_ring.mate_far()
     project_vg(3, 4)
     hsend[...] = ext[pl.ds(T, HALO), :].astype(BF16)
     h_k = w.new()
-    w.start(h_k, hsend, hrecv, following)
-    each(p2, 1, "near", "far")
+    w.start(5, h_k, hsend, hrecv, following)
+    p2[2].relay()
+    p2[3].first()
+    p2[1].rest()
     project_all(1, finish_fi)
+    p1[5].relay()
     local_states()
-    y_k = [w.new() for _ in range(3)]
-    z_k = [w.new() for _ in range(3)]
+    y_k, z_k = w.new(), w.new()
     for i in range(3):
-        w.start(y_k[i], sty.at[y], sty.at[y], at(z, y + 1 + i))
-
-    each(p1, 3, "relay")
-    each(p1, 4, "relay")
+        w.start(6, y_k, sty.at[y], sty.at[y], at(z, y + 1 + i))
+
+    p2[3].second()
     w.arrive(h_k, hrecv, preceding)
     convolve()
     conv_ring.start()
-    each(p1, 3, "near", "far")
-    each(p2, 3, "start")
-    each(p2, 2, "near", "far")
+    p2[2].rest()
     project_all(2, finish_qo)
-
-    for i in range(3):
-        w.arrive(y_k[i], sty.at[lax.rem(y + 3 - i, 4)], at(z, y + 1 + i))
+    p2[3].relay()
+    p2[4].first()
+
+    w.arrive(y_k, sty.at[pl.ds(0, 3)], at(z, y + 1))
     row_decay, row_state = jnp.ones((1, HEAD), F32), jnp.zeros((HEAD, HEAD), F32)
     my_decay, my_state = row_decay, row_state
     for i in range(4):
@@ -434,18 +436,16 @@
             my_state = jnp.where(take, row_state, my_state)
     pack_block(stz, z, row_decay, row_state)
     for i in range(3):
-        w.start(z_k[i], stz.at[z], stz.at[z], at(z + 1 + i, y))
-
-    each(p1, 4, "near", "far")
+        w.start(7, z_k, stz.at[z], stz.at[z], at(z + 1 + i, y))
+
+    p2[4].second()
     local_outputs()
-    each(p2, 3, "relay")
-    each(p2, 4, "start")
-    swapped()
-    each(p1, 5, "start")
     conv_ring.relay()
-
-    for i in range(3):
-        w.arrive(z_k[i], stz.at[lax.rem(z + 3 - i, 4)], at(z + 1 + i, y))
+    p1[5].rest()
+    p2[4].relay()
+    p2[5].first()
+
+    w.arrive(z_k, stz.at[pl.ds(0, 3)], at(z + 1, y))
     entering = siv[...].T
     for i in range(3):
         d, v = block_of(stz, i)
@@ -461,16 +461,14 @@
 
     lax.fori_loop(0, T // RT, finish_head, 0)
     rec_ring.start()
-    each(p1, 5, "relay")
-    each(p2, 4, "relay")
+    p2[5].second()
     conv_ring.near()
-    each(p2, 3, "near", "far")
+    p2[3].rest()
     project_all(3, finish_gate(sgr))
-    each(p1, 5, "near", "far")
-    each(p2, 5, "start")
     conv_ring.far()
+    conv_ring.mate_near()
+    p2[5].relay()
     rec_ring.relay()
-    conv_ring.mate_near()
     conv_ring.mate_far()
 
     gains, biases = [], []
@@ -496,11 +494,10 @@
 
     lax.fori_loop(0, T // 64, conv_scale, 0, unroll=4)
     lax.fori_loop(0, T // 64, normalize_conv, 0, unroll=2)
-    each(p2, 5, "relay")
     rec_ring.near()
-    each(p2, 4, "near", "far")
+    p2[4].rest()
     project_all(4, finish_gate(sgc))
-    each(p2, 5, "near", "far")
+    p2[5].rest()
     w_rec, w_conv = out_weight(10), out_weight(11)
 
     def conv_tile(r, _):
@@ -520,8 +517,14 @@
         return 0
 
     lax.fori_loop(0, T // RT, last_tile, 0)
-    for copy in w.sent:
-        copy.wait_send()
+    w.left(0, wb.at[pl.ds(0, 3), pl.ds(0, 3)], mate)
+    w.left(8, wb.at[pl.ds(0, 9)], mate)
+    w.left(1, xs.at[pl.ds(0, 7 * TD), :], mate)
+    w.left(2, mc.at[pl.ds(0, 7)], mate)
+    w.left(3, mr.at[pl.ds(0, 7)], mate)
+    w.left(5, hsend, following)
+    w.left(6, sty.at[pl.ds(0, 3)], mate)
+    w.left(7, stz.at[pl.ds(0, 3)], mate)
 
 
 def local(
@@ -543,7 +546,7 @@
         v((T + HALO, 128), F32), v((HALO, 128), BF16), v((HALO, 128), BF16), v((T, 256), F32), v((T, 256), F32),
         v((8, T + 16, 128), BF16), v((T, CONV), BF16), v((8, T, 128), BF16), v((T, 128), F32), v((T, 128), BF16),
         v((NC, 128, 128), BF16), v((16, 128), F32), v((4, 144, 128), BF16), v((4, 144, 128), BF16), v((NC, 128, 128), F32), v((T, 128), F32),
-        pltpu.SemaphoreType.DMA((24,)), pltpu.SemaphoreType.DMA((200,)), pltpu.SemaphoreType.DMA((200,)),
+        pltpu.SemaphoreType.DMA((10,)), pltpu.SemaphoreType.DMA((9,)), pltpu.SemaphoreType.DMA((43,)),
     ]
     return pl.pallas_call(
         kernel,
@@ -552,9 +555,9 @@
         out_specs=pl.BlockSpec(memory_space=pltpu.VMEM),
         scratch_shapes=scratch,
         compiler_params=pltpu.CompilerParams(
-            collective_id=0, has_side_effects=True, vmem_limit_bytes=56 * 1024 * 1024
+            collective_id=0, has_side_effects=True, vmem_limit_bytes=40 * 1024 * 1024
         ),
-    )(*args)
+    )(*[pltpu.with_memory_space_constraint(a, pltpu.HBM) for a in args])
 
 
 def solution(mesh):

time: 67.1 us -> 56.8 us (0.85)
  Pallas kernels: 65.2 us -> 55.9 us
  local copies, waits for them, and re-layouts: 1.77 us -> 0.75 us
    pallas_call x1, Pallas kernels: 65.2 us -> 55.9 us  [local(): pl.pallas_call(kernel, out_shape=jax.ShapeDtypeStruct((T, 256), BF16), in...]
    unnamed x1, local copies, waits for them, and re-layouts: 1.77 us -> 0.75 us
where the time goes in v4:
time: 56.8 us; the launch traced here: 56.7 us
  Pallas kernels  55.9 us (98%)
  local copies, waits for them, and re-layouts  0.75 us (1%)
    pallas_call x1, Pallas kernels, local(): pl.pallas_call(kernel, out_shape=jax.ShapeDtypeStruct((T, 256), BF16), in...  55.9 us

profile of v4, /device:TPU:1, one launch (start us, length us, event | category | flops | bytes accessed | tf_op | source)
XLA Modules:
  0.0 56.7 jit_solution(2536192706107860373)
XLA Ops:
  0.0 55.9 %shard_map.181 = bf16[768,256]{1,0:T(8,128)(2,1)S(1)} custom-call(bf16[96,2048]{1,0:T(8,128)(2,1)} %tokens.1, f32[1,2048]{1,0:T(1,128)} %bitcast.5, bf16[128,128]{1,0:T(8,128)(2,1)} %w_f.1, bf16[128,128]{1,0:T(8,128)(2,1)} %w_i.1, bf16[128,128]{1,0:T(8,128)(2,1)} %w_q.1, bf16[128,128]{1,0:T(8,128)(2,1)} %w_o.1, bf16[128,128]{1,0:T(8,128)(2,1)} %w_v.1, ...), custom_call_target="tpu_custom_call" | custom-call | tf_op jit(solution)/shard_map/pallas_call | solution.py:551
  55.9 0.7 %copy.21 = bf16[768,256]{1,0:T(8,128)(2,1)} copy(bf16[768,256]{1,0:T(8,128)(2,1)S(1)} %shard_map.181) | data formatting | bytes 786432

commit v5 on v4

--- a/solution.py
+++ b/solution.py
@@ -195,20 +195,6 @@
     def _():
         pl.semaphore_signal(barrier, inc=1, device_id=swap, device_id_type=MESH)
 
-    for copy in first:
-        copy.wait()
-    base = pl.multiple_of(t * TD, 16)
-
-    def normalize(r, _):
-        wide = tok[pl.ds(pl.multiple_of(r * 16, 16), 16), :].astype(F32)
-        scale = lax.rsqrt(jnp.mean(wide * wide, axis=-1, keepdims=True) + EPS)
-        xs[pl.ds(pl.multiple_of(base + r * 16, 16), 16), :] = (wide * scale * gainv[...]).astype(BF16)
-        return 0
-
-    lax.fori_loop(0, TD // 16, normalize, 0)
-    own.wait()
-    pl.semaphore_wait(barrier, len(partners) + jnp.where(home, 0, 1))
-
     def row_part(core):
         return lambda xx, h: xs.at[pl.ds(pl.multiple_of((xx * 2 + core) * TD + h * (TD // 2), 16), TD // 2), :]
 
@@ -242,9 +228,11 @@
         ]
         p2.append(Exchange(w, 8, rings, lambda n, b=a: wb.at[b, pl.ds(0, n)]))
 
-    for g in range(5):
+    stz[...] = jnp.zeros_like(stz)
+    own.wait()
+    pl.semaphore_wait(barrier, len(partners) + jnp.where(home, 0, 1))
+    for g in range(3):
         p1[g].start()
-    token_ring.start()
     swap_k = w.new()
 
     def place(i):
@@ -269,6 +257,19 @@
         @pl.when(home)
         def _():
             pltpu.make_async_copy(stage, stage, recv_sem.at[swap_k]).wait()
+
+    for copy in first:
+        copy.wait()
+    base = pl.multiple_of(t * TD, 16)
+
+    def normalize(r, _):
+        wide = tok[pl.ds(pl.multiple_of(r * 16, 16), 16), :].astype(F32)
+        scale = lax.rsqrt(jnp.mean(wide * wide, axis=-1, keepdims=True) + EPS)
+        xs[pl.ds(pl.multiple_of(base + r * 16, 16), 16), :] = (wide * scale * gainv[...]).astype(BF16)
+        return 0
+
+    lax.fori_loop(0, TD // 16, normalize, 0, unroll=TD // 16)
+    token_ring.start()
 
     def whole(b):
         return wb[b].reshape(2048, 128)
@@ -373,57 +374,51 @@
 
     p1[0].relay()
     p1[1].relay()
+    p1[3].start()
+    p1[4].start()
     p1[2].relay()
-    p1[3].relay()
-    p1[4].relay()
     p1[0].rest()
-    p2[0].first()
-    p2[0].second()
+    p2[0].start()
     p1[1].rest()
     p2[1].first()
     token_ring.relay()
-    p1[2].rest()
-    p1[3].rest()
-    p1[4].rest()
     p2[0].relay()
     p2[1].second()
     token_ring.near()
+    p1[2].rest()
     p2[1].relay()
     p2[2].first()
+    p1[3].relay()
+    p1[4].relay()
+    swapped()
+    p1[5].start()
     for copy in rest:
         copy.wait()
+    token_ring.far()
     p2[0].rest()
+    p2[2].second()
     token_ring.mate_near()
     project_vg = project(0, finish_vg, XT, by_ring)
     project_vg(0, 3)
-    p2[2].second()
-    swapped()
-    p1[5].start()
-    token_ring.far()
     token_ring.mate_far()
     project_vg(3, 4)
     hsend[...] = ext[pl.ds(T, HALO), :].astype(BF16)
     h_k = w.new()
     w.start(5, h_k, hsend, hrecv, following)
-    p2[2].relay()
-    p2[3].first()
     p2[1].rest()
     project_all(1, finish_fi)
-    p1[5].relay()
     local_states()
     y_k, z_k = w.new(), w.new()
-    for i in range(3):
-        w.start(6, y_k, sty.at[y], sty.at[y], at(z, y + 1 + i))
-
-    p2[3].second()
+    for i in (2, 1, 3):
+        w.start(6, y_k, sty.at[y], sty.at[y], at(z, y + i))
+
+    p2[2].relay()
+    p1[3].rest()
+    p1[5].relay()
+    p2[3].first()
     w.arrive(h_k, hrecv, preceding)
     convolve()
     conv_ring.start()
-    p2[2].rest()
-    project_all(2, finish_qo)
-    p2[3].relay()
-    p2[4].first()
-
     w.arrive(y_k, sty.at[pl.ds(0, 3)], at(z, y + 1))
     row_decay, row_state = jnp.ones((1, HEAD), F32), jnp.zeros((HEAD, HEAD), F32)
     my_decay, my_state = row_decay, row_state
@@ -435,40 +430,54 @@
             my_decay = jnp.where(take, row_decay, my_decay)
             my_state = jnp.where(take, row_state, my_state)
     pack_block(stz, z, row_decay, row_state)
-    for i in range(3):
-        w.start(7, z_k, stz.at[z], stz.at[z], at(z + 1 + i, y))
-
+    for i in (2, 1, 3):
+
+        @pl.when(z + i < 4)
+        def _(i=i):
+            w.start(7, z_k, stz.at[z], stz.at[z], at(z + i, y))
+
+
+    p2[3].second()
+    p1[4].rest()
+    p2[4].first()
+    p2[2].rest()
+    project_all(2, finish_qo)
+    conv_ring.relay()
+    p2[3].relay()
     p2[4].second()
+    p1[5].rest()
+    p2[5].first()
     local_outputs()
-    conv_ring.relay()
-    p1[5].rest()
-    p2[4].relay()
-    p2[5].first()
-
-    w.arrive(z_k, stz.at[pl.ds(0, 3)], at(z + 1, y))
+    p2[5].second()
+    for i in (1, 2, 3):
+
+        @pl.when(z == i)
+        def _(i=i):
+            w.arrive(z_k, stz.at[pl.ds(0, i)], at(z + 1, y))
+
     entering = siv[...].T
     for i in range(3):
         d, v = block_of(stz, i)
         entering = jnp.where(i < z, d * entering + v, entering)
     entering = (my_decay * entering + my_state).astype(BF16)
 
-    def finish_head(r, _):
-        rows = pl.ds(pl.multiple_of(r * RT, RT), RT)
-        h = head[rows, :] + dot_last(qd[rows, :], entering)
-        h = h * lax.rsqrt(jnp.mean(h * h, axis=-1, keepdims=True) + EPS) * hgv[...]
-        mr[t, rows, :] = (h * ogb[rows, :]).astype(BF16)
-        return 0
-
-    lax.fori_loop(0, T // RT, finish_head, 0)
+    def finish_head(low, high):
+        for r in range(low, high):
+            rows = pl.ds(r * 128, 128)
+            h = head[rows, :] + dot_last(qd[rows, :], entering)
+            h = h * lax.rsqrt(jnp.mean(h * h, axis=-1, keepdims=True) + EPS) * hgv[...]
+            mr[t, rows, :] = (h * ogb[rows, :]).astype(BF16)
+
+    finish_head(0, T // 128)
     rec_ring.start()
-    p2[5].second()
     conv_ring.near()
+    p2[4].relay()
+    conv_ring.far()
+    conv_ring.mate_near()
     p2[3].rest()
     project_all(3, finish_gate(sgr))
-    conv_ring.far()
-    conv_ring.mate_near()
+    rec_ring.relay()
     p2[5].relay()
-    rec_ring.relay()
     conv_ring.mate_far()
 
     gains, biases = [], []
@@ -524,7 +533,11 @@
     w.left(3, mr.at[pl.ds(0, 7)], mate)
     w.left(5, hsend, following)
     w.left(6, sty.at[pl.ds(0, 3)], mate)
-    w.left(7, stz.at[pl.ds(0, 3)], mate)
+    for i in (1, 2, 3):
+
+        @pl.when(z == 3 - i)
+        def _(i=i):
+            w.left(7, stz.at[pl.ds(0, i)], mate)
 
 
 def local(

time: 56.8 us -> 53.8 us (0.947)
  Pallas kernels: 55.9 us -> 53 us
    pallas_call x1, Pallas kernels: 55.9 us -> 53 us  [local(): pl.pallas_call(kernel, out_shape=jax.ShapeDtypeStruct((T, 256), BF16), in...]
where the time goes in v5:
time: 53.8 us; the launch traced here: 53.7 us
  Pallas kernels  53 us (99%)
  local copies, waits for them, and re-layouts  0.75 us (1%)
    pallas_call x1, Pallas kernels, local(): pl.pallas_call(kernel, out_shape=jax.ShapeDtypeStruct((T, 256), BF16), in...  53 us

profile of v5, /device:TPU:1, one launch (start us, length us, event | category | flops | bytes accessed | tf_op | source)
XLA Modules:
  0.0 53.7 jit_solution(17230722128896443112)
XLA Ops:
  0.0 53.0 %shard_map.181 = bf16[768,256]{1,0:T(8,128)(2,1)S(1)} custom-call(bf16[96,2048]{1,0:T(8,128)(2,1)} %tokens.1, f32[1,2048]{1,0:T(1,128)} %bitcast.5, bf16[128,128]{1,0:T(8,128)(2,1)} %w_f.1, bf16[128,128]{1,0:T(8,128)(2,1)} %w_i.1, bf16[128,128]{1,0:T(8,128)(2,1)} %w_q.1, bf16[128,128]{1,0:T(8,128)(2,1)} %w_o.1, bf16[128,128]{1,0:T(8,128)(2,1)} %w_v.1, ...), custom_call_target="tpu_custom_call" | custom-call | tf_op jit(solution)/shard_map/pallas_call | solution.py:564
  53.0 0.7 %copy.21 = bf16[768,256]{1,0:T(8,128)(2,1)} copy(bf16[768,256]{1,0:T(8,128)(2,1)S(1)} %shard_map.181) | data formatting | bytes 786432

commit v6 on v5

--- a/solution.py
+++ b/solution.py
@@ -54,20 +54,12 @@
 
 
 class Exchange:
-    def __init__(self, wires, lane, rings, span, mate=None):
-        self.w, self.lane, self.rings, self.span, self.mate = wires, lane, rings, span, mate
-        self.k = {"relay": wires.new(), "near": wires.new()}
-        self.k["far"] = self.k["near"] if mate is None else wires.new()
-        if mate is not None:
-            self.k["mate_near"], self.k["mate_far"] = wires.new(), wires.new()
+    def __init__(self, wires, lane, rings, span):
+        self.w, self.lane, self.rings, self.span = wires, lane, rings, span
+        self.k = {"relay": wires.new(), "rest": wires.new()}
 
     def go(self, sem, view, dev):
         self.w.start(self.lane, self.k[sem], view, view, dev)
-
-    def to_mate(self, sem, *views):
-        if self.mate is not None:
-            for view in views:
-                self.go(sem, view, self.mate)
 
     def await_blocks(self, sem, n):
         self.w.arrive(self.k[sem], self.span(n * len(self.rings)), self.rings[0][1])
@@ -79,9 +71,8 @@
 
     def second(self):
         for pos, plus, minus, part in self.rings:
-            self.go("near", part(pos, 1), plus)
-            self.go("near", part(pos, 0), minus)
-            self.to_mate("mate_near", part(pos, 0), part(pos, 1))
+            self.go("rest", part(pos, 1), plus)
+            self.go("rest", part(pos, 0), minus)
 
     def start(self):
         self.first()
@@ -90,29 +81,67 @@
     def relay(self):
         self.await_blocks("relay", 1)
         for pos, plus, minus, part in self.rings:
-            left, right = part(lax.rem(pos + 3, 4), 0), part(lax.rem(pos + 1, 4), 1)
-            self.go("far", left, plus)
-            self.go("far", right, minus)
-            self.to_mate("mate_near", left, right)
+            self.go("rest", part(lax.rem(pos + 3, 4), 0), plus)
+            self.go("rest", part(lax.rem(pos + 1, 4), 1), minus)
+
+    def rest(self):
+        self.await_blocks("rest", 2)
+
+
+class ChipExchange:
+    def __init__(self, wires, lane, pos, plus, minus, mate, sizes, view, span):
+        self.w, self.lane, self.pos, self.plus, self.minus, self.mate = wires, lane, pos, plus, minus, mate
+        self.sizes, self.view, self.span = sizes, view, span
+        self.k = {n: wires.new() for n in ("relay0", "relay1", "near", "far0", "far1", "mate_near", "mate_far")}
+
+    def piece(self, shift, half, i):
+        row = sum(self.sizes[0]) * half + (self.sizes[half][0] if i else 0)
+        return self.view(lax.rem(self.pos + shift, 4), row, self.sizes[half][i])
+
+    def half(self, shift, half):
+        return self.view(lax.rem(self.pos + shift, 4), sum(self.sizes[0]) * half, sum(self.sizes[half]))
+
+    def go(self, sem, view, dev):
+        self.w.start(self.lane, self.k[sem], view, view, dev)
+
+    def take(self, sem, blocks, rows, dev):
+        self.w.arrive(self.k[sem], self.span(blocks, rows), dev)
+
+    def rows(self, i):
+        return self.sizes[0][i] + self.sizes[1][i]
+
+    def start(self):
+        for i in range(2):
+            self.go(f"relay{i}", self.piece(0, 0, i), self.plus)
+            self.go(f"relay{i}", self.piece(0, 1, i), self.minus)
+        self.go("near", self.half(0, 1), self.plus)
+        self.go("near", self.half(0, 0), self.minus)
+        for h in range(2):
+            self.go("mate_near", self.half(0, h), self.mate)
+
+    def relay(self, i):
+        self.take(f"relay{i}", 0, self.rows(i), self.plus)
+        left, right = self.piece(3, 0, i), self.piece(1, 1, i)
+        self.go(f"far{i}", left, self.plus)
+        self.go(f"far{i}", right, self.minus)
+        self.go("mate_near", left, self.mate)
+        self.go("mate_near", right, self.mate)
 
     def near(self):
-        self.await_blocks("near", 1)
-        for pos, plus, minus, part in self.rings:
-            self.to_mate("mate_near", part(lax.rem(pos + 3, 4), 1), part(lax.rem(pos + 1, 4), 0))
-
-    def far(self):
-        self.await_blocks("far", 1)
-        for pos, plus, minus, part in self.rings:
-            self.to_mate("mate_far", part(lax.rem(pos + 2, 4), 0), part(lax.rem(pos + 2, 4), 1))
-
-    def rest(self):
-        self.await_blocks("near", 2)
+        self.take("near", 1, 0, self.plus)
+        self.go("mate_near", self.half(3, 1), self.mate)
+        self.go("mate_near", self.half(1, 0), self.mate)
+
+    def far(self, i):
+        self.take(f"far{i}", 0, self.rows(i), self.plus)
+        self.go("mate_far", self.piece(2, 0, i), self.mate)
+        self.go("mate_far", self.piece(2, 1, i), self.mate)
 
     def mate_near(self):
-        self.w.arrive(self.k["mate_near"], self.span(3), self.mate)
+        self.take("mate_near", 3, 0, self.mate)
 
     def mate_far(self):
-        self.w.arrive(self.k["mate_far"], self.span(1), self.mate)
+        self.take("mate_far", 1, 0, self.mate)
 
 
 def dot(a, b):
@@ -195,18 +224,23 @@
     def _():
         pl.semaphore_signal(barrier, inc=1, device_id=swap, device_id_type=MESH)
 
-    def row_part(core):
-        return lambda xx, h: xs.at[pl.ds(pl.multiple_of((xx * 2 + core) * TD + h * (TD // 2), 16), TD // 2), :]
-
-    def half_of(buf, core):
-        return lambda xx, h: buf.at[xx * 2 + core, pl.ds(384 * h, 384 if h == 0 else buf.shape[1] - 384)]
-
-    def tp_exchange(lane, part, span):
-        return Exchange(w, lane, [(x, across(x + 1), across(x - 1), part)], span, mate)
-
-    token_ring = tp_exchange(1, row_part(c), lambda n: xs.at[pl.ds(0, TD * n), :])
-    conv_ring = tp_exchange(2, half_of(mc, c), lambda n: mc.at[pl.ds(0, n)])
-    rec_ring = tp_exchange(3, half_of(mr, c), lambda n: mr.at[pl.ds(0, n)])
+    def exchange(lane, sizes, view, span):
+        return ChipExchange(w, lane, x, across(x + 1), across(x - 1), mate, sizes, view, span)
+
+    def token_view(xx, row, rows):
+        return xs.at[pl.ds(pl.multiple_of((xx * 2 + c) * TD + row, 16), rows), :]
+
+    def block_view(buf):
+        return lambda xx, row, rows: buf.at[xx * 2 + c, pl.ds(row, rows)]
+
+    def block_span(buf):
+        return lambda blocks, rows: buf.at[0, pl.ds(0, rows)] if rows else buf.at[pl.ds(0, blocks)]
+
+    token_ring = exchange(
+        1, ((32, 16), (32, 16)), token_view, lambda blocks, rows: xs.at[pl.ds(0, blocks * TD + rows), :]
+    )
+    conv_ring = exchange(2, ((192, 192), (192, 208)), block_view(mc), block_span(mc))
+    rec_ring = exchange(3, ((192, 192), (192, 192)), block_view(mr), block_span(mr))
 
     def along_y(part):
         return (y, at(z, y + 1), at(z, y - 1), part)
@@ -356,15 +390,12 @@
             head[rows, :] = o
             qd[rows, :] = (q * jnp.exp(total + rbuf[pl.ds(i, 1), :])).astype(BF16)
 
-    def convolve():
-        ext[pl.ds(0, HALO), :] = jnp.where(s > 0, hrecv[...].astype(F32), 0.0)
-        for i in range(T // 128):
+    def convolve(low, high):
+        for i in range(low, high):
             acc = jnp.zeros((128, HEAD), F32)
             for j in range(KW):
                 acc = acc + ckv[pl.ds(j, 1), :] * ext[pl.ds(i * 128 + HALO - KW + 1 + j, 128), :]
             mc[t, pl.ds(i * 128, 128), :] = acc.astype(BF16)
-        extra = [a.astype(F32) for v in (cgv[...], cbv[...]) for a in two(v)]
-        mc[t, pl.ds(T, 16), :] = jnp.concatenate(extra + [jnp.zeros((12, HEAD), F32)], axis=0).astype(BF16)
 
     def out_weight(b):
         sides = [
@@ -381,7 +412,8 @@
     p2[0].start()
     p1[1].rest()
     p2[1].first()
-    token_ring.relay()
+    token_ring.relay(0)
+    token_ring.relay(1)
     p2[0].relay()
     p2[1].second()
     token_ring.near()
@@ -394,7 +426,8 @@
     p1[5].start()
     for copy in rest:
         copy.wait()
-    token_ring.far()
+    token_ring.far(0)
+    token_ring.far(1)
     p2[0].rest()
     p2[2].second()
     token_ring.mate_near()
@@ -415,9 +448,13 @@
     p2[2].relay()
     p1[3].rest()
     p1[5].relay()
-    p2[3].first()
+    p2[3].start()
+    convolve(1, T // 128)
+    extra = [a.astype(F32) for v in (cgv[...], cbv[...]) for a in two(v)]
+    mc[t, pl.ds(T, 16), :] = jnp.concatenate(extra + [jnp.zeros((12, HEAD), F32)], axis=0).astype(BF16)
     w.arrive(h_k, hrecv, preceding)
-    convolve()
+    ext[pl.ds(0, HALO), :] = jnp.where(s > 0, hrecv[...].astype(F32), 0.0)
+    convolve(0, 1)
     conv_ring.start()
     w.arrive(y_k, sty.at[pl.ds(0, 3)], at(z, y + 1))
     row_decay, row_state = jnp.ones((1, HEAD), F32), jnp.zeros((HEAD, HEAD), F32)
@@ -437,18 +474,17 @@
             w.start(7, z_k, stz.at[z], stz.at[z], at(z + i, y))
 
 
-    p2[3].second()
     p1[4].rest()
     p2[4].first()
     p2[2].rest()
     project_all(2, finish_qo)
-    conv_ring.relay()
+    conv_ring.relay(0)
+    conv_ring.relay(1)
     p2[3].relay()
     p2[4].second()
+    local_outputs()
     p1[5].rest()
-    p2[5].first()
-    local_outputs()
-    p2[5].second()
+    p2[5].start()
     for i in (1, 2, 3):
 
         @pl.when(z == i)
@@ -472,13 +508,15 @@
     rec_ring.start()
     conv_ring.near()
     p2[4].relay()
-    conv_ring.far()
-    conv_ring.mate_near()
     p2[3].rest()
     project_all(3, finish_gate(sgr))
-    rec_ring.relay()
+    conv_ring.far(0)
+    conv_ring.far(1)
+    rec_ring.relay(0)
     p2[5].relay()
+    conv_ring.mate_near()
     conv_ring.mate_far()
+    rec_ring.relay(1)
 
     gains, biases = [], []
     for k in range(8):
@@ -506,6 +544,8 @@
     rec_ring.near()
     p2[4].rest()
     project_all(4, finish_gate(sgc))
+    rec_ring.far(0)
+    rec_ring.far(1)
     p2[5].rest()
     w_rec, w_conv = out_weight(10), out_weight(11)
 
@@ -515,7 +555,6 @@
         return 0
 
     lax.fori_loop(0, T // RT, conv_tile, 0)
-    rec_ring.far()
     rec_ring.mate_near()
     rec_ring.mate_far()
 
@@ -559,7 +598,7 @@
         v((T + HALO, 128), F32), v((HALO, 128), BF16), v((HALO, 128), BF16), v((T, 256), F32), v((T, 256), F32),
         v((8, T + 16, 128), BF16), v((T, CONV), BF16), v((8, T, 128), BF16), v((T, 128), F32), v((T, 128), BF16),
         v((NC, 128, 128), BF16), v((16, 128), F32), v((4, 144, 128), BF16), v((4, 144, 128), BF16), v((NC, 128, 128), F32), v((T, 128), F32),
-        pltpu.SemaphoreType.DMA((10,)), pltpu.SemaphoreType.DMA((9,)), pltpu.SemaphoreType.DMA((43,)),
+        pltpu.SemaphoreType.DMA((10,)), pltpu.SemaphoreType.DMA((9,)), pltpu.SemaphoreType.DMA((49,)),
     ]
     return pl.pallas_call(
         kernel,

time: 53.8 us -> 51.5 us (0.957)
  Pallas kernels: 53 us -> 50.6 us
    pallas_call x1, Pallas kernels: 53 us -> 50.6 us  [local(): pl.pallas_call(kernel, out_shape=jax.ShapeDtypeStruct((T, 256), BF16), in...]
where the time goes in v6:
time: 51.5 us; the launch traced here: 51.3 us
  Pallas kernels  50.6 us (98%)
  local copies, waits for them, and re-layouts  0.75 us (1%)
    pallas_call x1, Pallas kernels, local(): pl.pallas_call(kernel, out_shape=jax.ShapeDtypeStruct((T, 256), BF16), in...  50.6 us

profile of v6, /device:TPU:1, one launch (start us, length us, event | category | flops | bytes accessed | tf_op | source)
XLA Modules:
  0.0 51.3 jit_solution(6314847474429233412)
XLA Ops:
  0.0 50.6 %shard_map.181 = bf16[768,256]{1,0:T(8,128)(2,1)S(1)} custom-call(bf16[96,2048]{1,0:T(8,128)(2,1)} %tokens.1, f32[1,2048]{1,0:T(1,128)} %bitcast.5, bf16[128,128]{1,0:T(8,128)(2,1)} %w_f.1, bf16[128,128]{1,0:T(8,128)(2,1)} %w_i.1, bf16[128,128]{1,0:T(8,128)(2,1)} %w_q.1, bf16[128,128]{1,0:T(8,128)(2,1)} %w_o.1, bf16[128,128]{1,0:T(8,128)(2,1)} %w_v.1, ...), custom_call_target="tpu_custom_call" | custom-call | tf_op jit(solution)/shard_map/pallas_call | solution.py:603
  50.6 0.7 %copy.21 = bf16[768,256]{1,0:T(8,128)(2,1)} copy(bf16[768,256]{1,0:T(8,128)(2,1)S(1)} %shard_map.181) | data formatting | bytes 786432

commit v7 on v6

--- a/solution.py
+++ b/solution.py
@@ -169,7 +169,7 @@
     tokens, gain, w_f, w_i, w_q, w_o, w_v, w_g, w_gr, w_gc, lb, shift, sinit, hgain, ck, cgain, cbias, w_or, w_oc,
     out,
     tok, gainv, xs, wb, stage, lbv, shv, siv, hgv, ckv, cgv, cbv,
-    kgb, cb, vb, qb, ogb, ext, hsend, hrecv, sgr, sgc, mc, mcn, mr, head, qd, stb, rbuf, sty, stz, kv, scales,
+    kgb, cb, vb, qb, ogb, ext, hsend, hrecv, sgr, sgc, mc, mcn, mr, head, qd, stb, rbuf, sty, stz, kv, scales, acc,
     load_sem, send_sem, recv_sem,
 ):
     s, t = lax.axis_index("sp"), lax.axis_index("tp")
@@ -267,7 +267,7 @@
     pl.semaphore_wait(barrier, len(partners) + jnp.where(home, 0, 1))
     for g in range(3):
         p1[g].start()
-    swap_k = w.new()
+    swap_k, y_k, z_k, h_k = (w.new() for _ in range(4))
 
     def place(i):
         return wb.at[10 + i, swap[0] // 4, lax.rem(swap[0], 4)]
@@ -397,11 +397,19 @@
                 acc = acc + ckv[pl.ds(j, 1), :] * ext[pl.ds(i * 128 + HALO - KW + 1 + j, 128), :]
             mc[t, pl.ds(i * 128, 128), :] = acc.astype(BF16)
 
-    def out_weight(b):
-        sides = [
-            jnp.concatenate([wb[b, k // 2, (k % 2) * 2 + j] for k in range(8)], axis=0) for j in range(2)
-        ]
-        return jnp.concatenate(sides, axis=1)
+    def take_z():
+        for i in (1, 2, 3):
+
+            @pl.when(z == i)
+            def _(i=i):
+                w.arrive(z_k, stz.at[pl.ds(0, i)], at(z + 1, y))
+
+    def chip_weight(b, xx):
+        top, low = ([wb[b, xx, 2 * k + j] for j in range(2)] for k in range(2))
+        return jnp.concatenate([jnp.concatenate(top, axis=1), jnp.concatenate(low, axis=1)], axis=0)
+
+    def chip_blocks(rows, xx):
+        return jnp.concatenate([mr[2 * xx, rows, :], mr[2 * xx + 1, rows, :]], axis=1)
 
     p1[0].relay()
     p1[1].relay()
@@ -436,12 +444,10 @@
     token_ring.mate_far()
     project_vg(3, 4)
     hsend[...] = ext[pl.ds(T, HALO), :].astype(BF16)
-    h_k = w.new()
     w.start(5, h_k, hsend, hrecv, following)
     p2[1].rest()
     project_all(1, finish_fi)
     local_states()
-    y_k, z_k = w.new(), w.new()
     for i in (2, 1, 3):
         w.start(6, y_k, sty.at[y], sty.at[y], at(z, y + i))
 
@@ -485,12 +491,7 @@
     local_outputs()
     p1[5].rest()
     p2[5].start()
-    for i in (1, 2, 3):
-
-        @pl.when(z == i)
-        def _(i=i):
-            w.arrive(z_k, stz.at[pl.ds(0, i)], at(z + 1, y))
-
+    take_z()
     entering = siv[...].T
     for i in range(3):
         d, v = block_of(stz, i)
@@ -513,10 +514,10 @@
     conv_ring.far(0)
     conv_ring.far(1)
     rec_ring.relay(0)
+    rec_ring.relay(1)
     p2[5].relay()
     conv_ring.mate_near()
     conv_ring.mate_far()
-    rec_ring.relay(1)
 
     gains, biases = [], []
     for k in range(8):
@@ -547,21 +548,32 @@
     rec_ring.far(0)
     rec_ring.far(1)
     p2[5].rest()
-    w_rec, w_conv = out_weight(10), out_weight(11)
+    w_conv = jnp.concatenate([chip_weight(11, xx) for xx in range(4)], axis=0)
 
     def conv_tile(r, _):
-        rows = pl.ds(pl.multiple_of(r * RT, RT), RT)
+        rows = pl.ds(pl.multiple_of(r * PT, PT), PT)
         sgc[rows, :] = sgc[rows, :] * rounded(dot(mcn[rows, :], w_conv))
         return 0
 
-    lax.fori_loop(0, T // RT, conv_tile, 0)
+    lax.fori_loop(0, T // PT, conv_tile, 0)
     rec_ring.mate_near()
+    near = [x, lax.rem(x + 1, 4), lax.rem(x + 3, 4)]
+    w_near = jnp.concatenate([chip_weight(10, xx) for xx in near], axis=0)
+
+    def near_tile(r, _):
+        rows = pl.ds(pl.multiple_of(r * PT, PT), PT)
+        acc[rows, :] = dot(jnp.concatenate([chip_blocks(rows, xx) for xx in near], axis=1), w_near)
+        return 0
+
+    lax.fori_loop(0, T // PT, near_tile, 0)
     rec_ring.mate_far()
+    opposite = lax.rem(x + 2, 4)
+    w_far = chip_weight(10, opposite)
 
     def last_tile(r, _):
         rows = pl.ds(pl.multiple_of(r * RT, RT), RT)
-        mixed = jnp.concatenate([mr[k, rows, :] for k in range(8)], axis=1)
-        out[rows, :] = (sgr[rows, :] * rounded(dot(mixed, w_rec)) + sgc[rows, :]).astype(BF16)
+        y_rec = rounded(acc[rows, :] + dot(chip_blocks(rows, opposite), w_far))
+        out[rows, :] = (sgr[rows, :] * y_rec + sgc[rows, :]).astype(BF16)
         return 0
 
     lax.fori_loop(0, T // RT, last_tile, 0)
@@ -597,7 +609,7 @@
         v((T, 128), F32), v((T, 128), F32), v((T, 128), BF16), v((T, 128), F32), v((T, 128), F32),
         v((T + HALO, 128), F32), v((HALO, 128), BF16), v((HALO, 128), BF16), v((T, 256), F32), v((T, 256), F32),
         v((8, T + 16, 128), BF16), v((T, CONV), BF16), v((8, T, 128), BF16), v((T, 128), F32), v((T, 128), BF16),
-        v((NC, 128, 128), BF16), v((16, 128), F32), v((4, 144, 128), BF16), v((4, 144, 128), BF16), v((NC, 128, 128), F32), v((T, 128), F32),
+        v((NC, 128, 128), BF16), v((16, 128), F32), v((4, 144, 128), BF16), v((4, 144, 128), BF16), v((NC, 128, 128), F32), v((T, 128), F32), v((T, 256), F32),
         pltpu.SemaphoreType.DMA((10,)), pltpu.SemaphoreType.DMA((9,)), pltpu.SemaphoreType.DMA((49,)),
     ]
     return pl.pallas_call(

time: 51.5 us -> 51.6 us (level); the launches traced: 51.3 us -> 50.9 us
  no operation moved by 1% of the time
where the time goes in v7:
time: 51.6 us; the launch traced here: 50.9 us
  Pallas kernels  50.1 us (97%)
  local copies, waits for them, and re-layouts  0.75 us (1%)
    pallas_call x1, Pallas kernels, local(): pl.pallas_call(kernel, out_shape=jax.ShapeDtypeStruct((T, 256), BF16), in...  50.1 us

profile of v7, /device:TPU:1, one launch (start us, length us, event | category | flops | bytes accessed | tf_op | source)
XLA Modules:
  0.0 50.9 jit_solution(4292186492192304297)
XLA Ops:
  0.0 50.1 %shard_map.181 = bf16[768,256]{1,0:T(8,128)(2,1)S(1)} custom-call(bf16[96,2048]{1,0:T(8,128)(2,1)} %tokens.1, f32[1,2048]{1,0:T(1,128)} %bitcast.5, bf16[128,128]{1,0:T(8,128)(2,1)} %w_f.1, bf16[128,128]{1,0:T(8,128)(2,1)} %w_i.1, bf16[128,128]{1,0:T(8,128)(2,1)} %w_q.1, bf16[128,128]{1,0:T(8,128)(2,1)} %w_o.1, bf16[128,128]{1,0:T(8,128)(2,1)} %w_v.1, ...), custom_call_target="tpu_custom_call" | custom-call | tf_op jit(solution)/shard_map/pallas_call | solution.py:615
  50.2 0.7 %copy.21 = bf16[768,256]{1,0:T(8,128)(2,1)} copy(bf16[768,256]{1,0:T(8,128)(2,1)S(1)} %shard_map.181) | data formatting | bytes 786432

commit v8 on v7

--- a/solution.py
+++ b/solution.py
@@ -317,7 +317,10 @@
             finish(start, rows, dot(xs[rows, :], weight))
             return 0
 
-        return lambda low, high: lax.fori_loop(low, high, tile, 0)
+        def run(low, high):
+            lax.fori_loop(low, high, tile, 0, unroll=high - low if high - low > 1 else None)
+
+        return run
 
     def project_all(group, finish):
         project(group, finish, PT, lambda r: r * PT)(0, T // PT)
@@ -509,21 +512,14 @@
     rec_ring.start()
     conv_ring.near()
     p2[4].relay()
-    p2[3].rest()
-    project_all(3, finish_gate(sgr))
     conv_ring.far(0)
     conv_ring.far(1)
+    p2[3].rest()
+    project_gr = project(3, finish_gate(sgr), PT, lambda r: r * PT)
+    project_gr(0, 1)
     rec_ring.relay(0)
-    rec_ring.relay(1)
-    p2[5].relay()
     conv_ring.mate_near()
     conv_ring.mate_far()
-
-    gains, biases = [], []
-    for k in range(8):
-        four = mc[k, pl.ds(T, 16), :].astype(F32)
-        gains.append(0.5 * (four[0:1, :] + four[1:2, :]))
-        biases.append(0.5 * (four[2:3, :] + four[3:4, :]))
 
     def conv_scale(r, _):
         rows = pl.ds(pl.multiple_of(r * 64, 64), 64)
@@ -531,6 +527,12 @@
         scale = lax.rsqrt(jnp.sum(squares, axis=-1, keepdims=True) * (1.0 / CONV) + EPS)
         scales[rows, :] = jnp.broadcast_to(scale, (64, 128))
         return 0
+
+    gains, biases = [], []
+    for k in range(8):
+        four = mc[k, pl.ds(T, 16), :].astype(F32)
+        gains.append(0.5 * (four[0:1, :] + four[1:2, :]))
+        biases.append(0.5 * (four[2:3, :] + four[3:4, :]))
 
     def normalize_conv(r, _):
         rows = pl.ds(pl.multiple_of(r * 64, 64), 64)
@@ -541,6 +543,9 @@
         return 0
 
     lax.fori_loop(0, T // 64, conv_scale, 0, unroll=4)
+    rec_ring.relay(1)
+    p2[5].relay()
+    project_gr(1, 2)
     lax.fori_loop(0, T // 64, normalize_conv, 0, unroll=2)
     rec_ring.near()
     p2[4].rest()
@@ -555,7 +560,7 @@
         sgc[rows, :] = sgc[rows, :] * rounded(dot(mcn[rows, :], w_conv))
         return 0
 
-    lax.fori_loop(0, T // PT, conv_tile, 0)
+    lax.fori_loop(0, T // PT, conv_tile, 0, unroll=2)
     rec_ring.mate_near()
     near = [x, lax.rem(x + 1, 4), lax.rem(x + 3, 4)]
     w_near = jnp.concatenate([chip_weight(10, xx) for xx in near], axis=0)
@@ -565,7 +570,7 @@
         acc[rows, :] = dot(jnp.concatenate([chip_blocks(rows, xx) for xx in near], axis=1), w_near)
         return 0
 
-    lax.fori_loop(0, T // PT, near_tile, 0)
+    lax.fori_loop(0, T // PT, near_tile, 0, unroll=2)
     rec_ring.mate_far()
     opposite = lax.rem(x + 2, 4)
     w_far = chip_weight(10, opposite)
@@ -576,7 +581,7 @@
         out[rows, :] = (sgr[rows, :] * y_rec + sgc[rows, :]).astype(BF16)
         return 0
 
-    lax.fori_loop(0, T // RT, last_tile, 0)
+    lax.fori_loop(0, T // RT, last_tile, 0, unroll=3)
     w.left(0, wb.at[pl.ds(0, 3), pl.ds(0, 3)], mate)
     w.left(8, wb.at[pl.ds(0, 9)], mate)
     w.left(1, xs.at[pl.ds(0, 7 * TD), :], mate)

time: 51.6 us -> 50.8 us (0.984); the launches traced: 50.9 us -> 50.7 us
  no operation moved by 1% of the time
where the time goes in v8:
time: 50.8 us; the launch traced here: 50.7 us
  Pallas kernels  49.9 us (98%)
  local copies, waits for them, and re-layouts  0.75 us (1%)
    pallas_call x1, Pallas kernels, local(): pl.pallas_call(kernel, out_shape=jax.ShapeDtypeStruct((T, 256), BF16), in...  49.9 us

profile of v8, /device:TPU:1, one launch (start us, length us, event | category | flops | bytes accessed | tf_op | source)
XLA Modules:
  0.0 50.7 jit_solution(7389871901340904046)
XLA Ops:
  0.0 49.9 %shard_map.181 = bf16[768,256]{1,0:T(8,128)(2,1)S(1)} custom-call(bf16[96,2048]{1,0:T(8,128)(2,1)} %tokens.1, f32[1,2048]{1,0:T(1,128)} %bitcast.5, bf16[128,128]{1,0:T(8,128)(2,1)} %w_f.1, bf16[128,128]{1,0:T(8,128)(2,1)} %w_i.1, bf16[128,128]{1,0:T(8,128)(2,1)} %w_q.1, bf16[128,128]{1,0:T(8,128)(2,1)} %w_o.1, bf16[128,128]{1,0:T(8,128)(2,1)} %w_v.1, ...), custom_call_target="tpu_custom_call" | custom-call | tf_op jit(solution)/shard_map/pallas_call | solution.py:620
  49.9 0.7 %copy.21 = bf16[768,256]{1,0:T(8,128)(2,1)} copy(bf16[768,256]{1,0:T(8,128)(2,1)S(1)} %shard_map.181) | data formatting | bytes 786432

commit v9 on v8

--- a/solution.py
+++ b/solution.py
@@ -215,10 +215,15 @@
     ]
 
     barrier = pltpu.get_barrier_semaphore()
-    partners = [at(z, y + 1), at(z, y - 1), at(z, y + 2), at(z + 1, y), at(z - 1, y), at(z + 2, y)]
-    partners += [across(x + 1), across(x - 1), mate, following, preceding]
+    partners = [at(z, y + 1), at(z, y - 1), at(z + 1, y), at(z - 1, y), across(x + 1), across(x - 1), mate]
     for dev in partners:
         pl.semaphore_signal(barrier, inc=1, device_id=dev, device_id_type=MESH)
+
+    for there, dev in ((s < 15, following), (s > 0, preceding)):
+
+        @pl.when(there)
+        def _(dev=dev):
+            pl.semaphore_signal(barrier, inc=1, device_id=dev, device_id_type=MESH)
 
     @pl.when(jnp.logical_not(home))
     def _():
@@ -264,7 +269,8 @@
 
     stz[...] = jnp.zeros_like(stz)
     own.wait()
-    pl.semaphore_wait(barrier, len(partners) + jnp.where(home, 0, 1))
+    count = len(partners) + jnp.where(home, 0, 1) + jnp.where(s < 15, 1, 0) + jnp.where(s > 0, 1, 0)
+    pl.semaphore_wait(barrier, count)
     for g in range(3):
         p1[g].start()
     swap_k, y_k, z_k, h_k = (w.new() for _ in range(4))
@@ -399,6 +405,16 @@
             for j in range(KW):
                 acc = acc + ckv[pl.ds(j, 1), :] * ext[pl.ds(i * 128 + HALO - KW + 1 + j, 128), :]
             mc[t, pl.ds(i * 128, 128), :] = acc.astype(BF16)
+
+    def take_halo():
+        @pl.when(s > 0)
+        def _():
+            w.arrive(h_k, hrecv, preceding)
+            ext[pl.ds(0, HALO), :] = hrecv[...].astype(F32)
+
+        @pl.when(s == 0)
+        def _():
+            ext[pl.ds(0, HALO), :] = jnp.zeros((HALO, HEAD), F32)
 
     def take_z():
         for i in (1, 2, 3):
@@ -447,7 +463,11 @@
     token_ring.mate_far()
     project_vg(3, 4)
     hsend[...] = ext[pl.ds(T, HALO), :].astype(BF16)
-    w.start(5, h_k, hsend, hrecv, following)
+
+    @pl.when(s < 15)
+    def _():
+        w.start(5, h_k, hsend, hrecv, following)
+
     p2[1].rest()
     project_all(1, finish_fi)
     local_states()
@@ -461,8 +481,7 @@
     convolve(1, T // 128)
     extra = [a.astype(F32) for v in (cgv[...], cbv[...]) for a in two(v)]
     mc[t, pl.ds(T, 16), :] = jnp.concatenate(extra + [jnp.zeros((12, HEAD), F32)], axis=0).astype(BF16)
-    w.arrive(h_k, hrecv, preceding)
-    ext[pl.ds(0, HALO), :] = jnp.where(s > 0, hrecv[...].astype(F32), 0.0)
+    take_halo()
     convolve(0, 1)
     conv_ring.start()
     w.arrive(y_k, sty.at[pl.ds(0, 3)], at(z, y + 1))
@@ -483,17 +502,17 @@
             w.start(7, z_k, stz.at[z], stz.at[z], at(z + i, y))
 
 
-    p1[4].rest()
-    p2[4].first()
+    p1[5].rest()
+    p2[5].first()
     p2[2].rest()
     project_all(2, finish_qo)
     conv_ring.relay(0)
     conv_ring.relay(1)
     p2[3].relay()
-    p2[4].second()
+    p2[5].second()
     local_outputs()
-    p1[5].rest()
-    p2[5].start()
+    p1[4].rest()
+    p2[4].start()
     take_z()
     entering = siv[...].T
     for i in range(3):
@@ -511,12 +530,9 @@
     finish_head(0, T // 128)
     rec_ring.start()
     conv_ring.near()
-    p2[4].relay()
+    p2[5].relay()
     conv_ring.far(0)
     conv_ring.far(1)
-    p2[3].rest()
-    project_gr = project(3, finish_gate(sgr), PT, lambda r: r * PT)
-    project_gr(0, 1)
     rec_ring.relay(0)
     conv_ring.mate_near()
     conv_ring.mate_far()
@@ -544,23 +560,22 @@
 
     lax.fori_loop(0, T // 64, conv_scale, 0, unroll=4)
     rec_ring.relay(1)
-    p2[5].relay()
-    project_gr(1, 2)
+    p2[4].relay()
+    p2[3].rest()
+    project_all(3, finish_gate(sgr))
+    rec_ring.near()
     lax.fori_loop(0, T // 64, normalize_conv, 0, unroll=2)
-    rec_ring.near()
-    p2[4].rest()
-    project_all(4, finish_gate(sgc))
+    p2[5].rest()
+    w_conv = jnp.concatenate([chip_weight(11, xx) for xx in range(4)], axis=0)
+
+    def conv_tile(r, _):
+        rows = pl.ds(pl.multiple_of(r * PT, PT), PT)
+        sgc[rows, :] = rounded(dot(mcn[rows, :], w_conv))
+        return 0
+
+    lax.fori_loop(0, T // PT, conv_tile, 0, unroll=2)
     rec_ring.far(0)
     rec_ring.far(1)
-    p2[5].rest()
-    w_conv = jnp.concatenate([chip_weight(11, xx) for xx in range(4)], axis=0)
-
-    def conv_tile(r, _):
-        rows = pl.ds(pl.multiple_of(r * PT, PT), PT)
-        sgc[rows, :] = sgc[rows, :] * rounded(dot(mcn[rows, :], w_conv))
-        return 0
-
-    lax.fori_loop(0, T // PT, conv_tile, 0, unroll=2)
     rec_ring.mate_near()
     near = [x, lax.rem(x + 1, 4), lax.rem(x + 3, 4)]
     w_near = jnp.concatenate([chip_weight(10, xx) for xx in near], axis=0)
@@ -571,6 +586,12 @@
         return 0
 
     lax.fori_loop(0, T // PT, near_tile, 0, unroll=2)
+    p2[4].rest()
+
+    def finish_gc(start, rows, v):
+        sgc[rows, :] = jax.nn.sigmoid(rounded(v)) * sgc[rows, :]
+
+    project_all(4, finish_gc)
     rec_ring.mate_far()
     opposite = lax.rem(x + 2, 4)
     w_far = chip_weight(10, opposite)
@@ -587,7 +608,11 @@
     w.left(1, xs.at[pl.ds(0, 7 * TD), :], mate)
     w.left(2, mc.at[pl.ds(0, 7)], mate)
     w.left(3, mr.at[pl.ds(0, 7)], mate)
-    w.left(5, hsend, following)
+
+    @pl.when(s < 15)
+    def _():
+        w.left(5, hsend, following)
+
     w.left(6, sty.at[pl.ds(0, 3)], mate)
     for i in (1, 2, 3):
 

time: 50.8 us -> 49.8 us (0.980)
  Pallas kernels: 49.9 us -> 48.9 us
    pallas_call x1, Pallas kernels: 49.9 us -> 48.9 us  [local(): pl.pallas_call(kernel, out_shape=jax.ShapeDtypeStruct((T, 256), BF16), in...]
where the time goes in v9:
time: 49.8 us; the launch traced here: 49.7 us
  Pallas kernels  48.9 us (98%)
  local copies, waits for them, and re-layouts  0.75 us (2%)
    pallas_call x1, Pallas kernels, local(): pl.pallas_call(kernel, out_shape=jax.ShapeDtypeStruct((T, 256), BF16), in...  48.9 us

profile of v9, /device:TPU:1, one launch (start us, length us, event | category | flops | bytes accessed | tf_op | source)
XLA Modules:
  0.0 49.7 jit_solution(2788480574139290797)
XLA Ops:
  0.0 48.9 %shard_map.181 = bf16[768,256]{1,0:T(8,128)(2,1)S(1)} custom-call(bf16[96,2048]{1,0:T(8,128)(2,1)} %tokens.1, f32[1,2048]{1,0:T(1,128)} %bitcast.5, bf16[128,128]{1,0:T(8,128)(2,1)} %w_f.1, bf16[128,128]{1,0:T(8,128)(2,1)} %w_i.1, bf16[128,128]{1,0:T(8,128)(2,1)} %w_q.1, bf16[128,128]{1,0:T(8,128)(2,1)} %w_o.1, bf16[128,128]{1,0:T(8,128)(2,1)} %w_v.1, ...), custom_call_target="tpu_custom_call" | custom-call | tf_op jit(solution)/shard_map/pallas_call | solution.py:645
  48.9 0.7 %copy.21 = bf16[768,256]{1,0:T(8,128)(2,1)} copy(bf16[768,256]{1,0:T(8,128)(2,1)S(1)} %shard_map.181) | data formatting | bytes 786432

commit v10 on v9

--- a/solution.py
+++ b/solution.py
@@ -54,9 +54,9 @@
 
 
 class Exchange:
-    def __init__(self, wires, lane, rings, span):
+    def __init__(self, wires, lane, rings, span, k=None):
         self.w, self.lane, self.rings, self.span = wires, lane, rings, span
-        self.k = {"relay": wires.new(), "rest": wires.new()}
+        self.k = k or {"relay": wires.new(), "rest": wires.new()}
 
     def go(self, sem, view, dev):
         self.w.start(self.lane, self.k[sem], view, view, dev)
@@ -89,10 +89,12 @@
 
 
 class ChipExchange:
-    def __init__(self, wires, lane, pos, plus, minus, mate, sizes, view, span):
+    def __init__(self, wires, lane, pos, plus, minus, mate, sizes, view, span, k=None):
         self.w, self.lane, self.pos, self.plus, self.minus, self.mate = wires, lane, pos, plus, minus, mate
         self.sizes, self.view, self.span = sizes, view, span
-        self.k = {n: wires.new() for n in ("relay0", "relay1", "near", "far0", "far1", "mate_near", "mate_far")}
+        names = ("relay0", "relay1", "near", "far0", "far1")
+        self.k = {n: k[n] if k else wires.new() for n in names}
+        self.k.update({n: wires.new() for n in ("mate_near", "mate_far")})
 
     def piece(self, shift, half, i):
         row = sum(self.sizes[0]) * half + (self.sizes[half][0] if i else 0)
@@ -219,7 +221,7 @@
     for dev in partners:
         pl.semaphore_signal(barrier, inc=1, device_id=dev, device_id_type=MESH)
 
-    for there, dev in ((s < 15, following), (s > 0, preceding)):
+    for there, dev in ((s > 0, preceding),):
 
         @pl.when(there)
         def _(dev=dev):
@@ -229,8 +231,8 @@
     def _():
         pl.semaphore_signal(barrier, inc=1, device_id=swap, device_id_type=MESH)
 
-    def exchange(lane, sizes, view, span):
-        return ChipExchange(w, lane, x, across(x + 1), across(x - 1), mate, sizes, view, span)
+    def exchange(lane, sizes, view, span, k=None):
+        return ChipExchange(w, lane, x, across(x + 1), across(x - 1), mate, sizes, view, span, k)
 
     def token_view(xx, row, rows):
         return xs.at[pl.ds(pl.multiple_of((xx * 2 + c) * TD + row, 16), rows), :]
@@ -245,7 +247,7 @@
         1, ((32, 16), (32, 16)), token_view, lambda blocks, rows: xs.at[pl.ds(0, blocks * TD + rows), :]
     )
     conv_ring = exchange(2, ((192, 192), (192, 208)), block_view(mc), block_span(mc))
-    rec_ring = exchange(3, ((192, 192), (192, 192)), block_view(mr), block_span(mr))
+    rec_ring = exchange(3, ((192, 192), (192, 192)), block_view(mr), block_span(mr), token_ring.k)
 
     def along_y(part):
         return (y, at(z, y + 1), at(z, y - 1), part)
@@ -265,11 +267,11 @@
             along_z(lambda p, h, b=a: wb.at[b, p, pl.ds(2 * h, 2)]),
             along_y(lambda p, h, b=b: wb.at[b, pl.ds(2 * h, 2), p]),
         ]
-        p2.append(Exchange(w, 8, rings, lambda n, b=a: wb.at[b, pl.ds(0, n)]))
+        p2.append(Exchange(w, 8, rings, lambda n, b=a: wb.at[b, pl.ds(0, n)], p1[g - 3].k if g > 2 else None))
 
     stz[...] = jnp.zeros_like(stz)
     own.wait()
-    count = len(partners) + jnp.where(home, 0, 1) + jnp.where(s < 15, 1, 0) + jnp.where(s > 0, 1, 0)
+    count = len(partners) + jnp.where(home, 0, 1) + jnp.where(s < 15, 1, 0)
     pl.semaphore_wait(barrier, count)
     for g in range(3):
         p1[g].start()
@@ -640,7 +642,7 @@
         v((T + HALO, 128), F32), v((HALO, 128), BF16), v((HALO, 128), BF16), v((T, 256), F32), v((T, 256), F32),
         v((8, T + 16, 128), BF16), v((T, CONV), BF16), v((8, T, 128), BF16), v((T, 128), F32), v((T, 128), BF16),
         v((NC, 128, 128), BF16), v((16, 128), F32), v((4, 144, 128), BF16), v((4, 144, 128), BF16), v((NC, 128, 128), F32), v((T, 128), F32), v((T, 256), F32),
-        pltpu.SemaphoreType.DMA((10,)), pltpu.SemaphoreType.DMA((9,)), pltpu.SemaphoreType.DMA((49,)),
+        pltpu.SemaphoreType.DMA((10,)), pltpu.SemaphoreType.DMA((9,)), pltpu.SemaphoreType.DMA((38,)),
     ]
     return pl.pallas_call(
         kernel,

time: 49.8 us -> 49.7 us (level)
  no operation moved by 1% of the time
where the time goes in v10:
time: 49.7 us; the launch traced here: 49.6 us
  Pallas kernels  48.8 us (98%)
  local copies, waits for them, and re-layouts  0.75 us (2%)
    pallas_call x1, Pallas kernels, local(): pl.pallas_call(kernel, out_shape=jax.ShapeDtypeStruct((T, 256), BF16), in...  48.8 us

profile of v10, /device:TPU:1, one launch (start us, length us, event | category | flops | bytes accessed | tf_op | source)
XLA Modules:
  0.0 49.6 jit_solution(12927971663081898503)
XLA Ops:
  0.0 48.8 %shard_map.181 = bf16[768,256]{1,0:T(8,128)(2,1)S(1)} custom-call(bf16[96,2048]{1,0:T(8,128)(2,1)} %tokens.1, f32[1,2048]{1,0:T(1,128)} %bitcast.5, bf16[128,128]{1,0:T(8,128)(2,1)} %w_f.1, bf16[128,128]{1,0:T(8,128)(2,1)} %w_i.1, bf16[128,128]{1,0:T(8,128)(2,1)} %w_q.1, bf16[128,128]{1,0:T(8,128)(2,1)} %w_o.1, bf16[128,128]{1,0:T(8,128)(2,1)} %w_v.1, ...), custom_call_target="tpu_custom_call" | custom-call | tf_op jit(solution)/shard_map/pallas_call | solution.py:647
  48.8 0.7 %copy.21 = bf16[768,256]{1,0:T(8,128)(2,1)} copy(bf16[768,256]{1,0:T(8,128)(2,1)S(1)} %shard_map.181) | data formatting | bytes 786432

commit v11 on v10

--- a/solution.py
+++ b/solution.py
@@ -113,9 +113,15 @@
         return self.sizes[0][i] + self.sizes[1][i]
 
     def start(self):
-        for i in range(2):
-            self.go(f"relay{i}", self.piece(0, 0, i), self.plus)
-            self.go(f"relay{i}", self.piece(0, 1, i), self.minus)
+        self.start_piece(0)
+        self.start_piece(1)
+        self.start_rest()
+
+    def start_piece(self, i):
+        self.go(f"relay{i}", self.piece(0, 0, i), self.plus)
+        self.go(f"relay{i}", self.piece(0, 1, i), self.minus)
+
+    def start_rest(self):
         self.go("near", self.half(0, 1), self.plus)
         self.go("near", self.half(0, 0), self.minus)
         for h in range(2):
@@ -522,15 +528,18 @@
         entering = jnp.where(i < z, d * entering + v, entering)
     entering = (my_decay * entering + my_state).astype(BF16)
 
-    def finish_head(low, high):
-        for r in range(low, high):
-            rows = pl.ds(r * 128, 128)
+    def finish_head(*starts):
+        for start in starts:
+            rows = pl.ds(start, 192)
             h = head[rows, :] + dot_last(qd[rows, :], entering)
             h = h * lax.rsqrt(jnp.mean(h * h, axis=-1, keepdims=True) + EPS) * hgv[...]
             mr[t, rows, :] = (h * ogb[rows, :]).astype(BF16)
 
-    finish_head(0, T // 128)
-    rec_ring.start()
+    finish_head(0, 384)
+    rec_ring.start_piece(0)
+    finish_head(192, 576)
+    rec_ring.start_piece(1)
+    rec_ring.start_rest()
     conv_ring.near()
     p2[5].relay()
     conv_ring.far(0)

time: 49.7 us -> 49.7 us (level)
  no operation moved by 1% of the time
where the time goes in v11:
time: 49.7 us; the launch traced here: 49.6 us
  Pallas kernels  48.8 us (98%)
  local copies, waits for them, and re-layouts  0.75 us (2%)
    pallas_call x1, Pallas kernels, local(): pl.pallas_call(kernel, out_shape=jax.ShapeDtypeStruct((T, 256), BF16), in...  48.8 us

profile of v11, /device:TPU:1, one launch (start us, length us, event | category | flops | bytes accessed | tf_op | source)
XLA Modules:
  0.0 49.6 jit_solution(3413358859050376219)
XLA Ops:
  0.0 48.8 %shard_map.181 = bf16[768,256]{1,0:T(8,128)(2,1)S(1)} custom-call(bf16[96,2048]{1,0:T(8,128)(2,1)} %tokens.1, f32[1,2048]{1,0:T(1,128)} %bitcast.5, bf16[128,128]{1,0:T(8,128)(2,1)} %w_f.1, bf16[128,128]{1,0:T(8,128)(2,1)} %w_i.1, bf16[128,128]{1,0:T(8,128)(2,1)} %w_q.1, bf16[128,128]{1,0:T(8,128)(2,1)} %w_o.1, bf16[128,128]{1,0:T(8,128)(2,1)} %w_v.1, ...), custom_call_target="tpu_custom_call" | custom-call | tf_op jit(solution)/shard_map/pallas_call | solution.py:656
  48.8 0.7 %copy.21 = bf16[768,256]{1,0:T(8,128)(2,1)} copy(bf16[768,256]{1,0:T(8,128)(2,1)S(1)} %shard_map.181) | data formatting | bytes 786432

commit v12 on v10

--- a/solution.py
+++ b/solution.py
@@ -270,6 +270,7 @@
         p2.append(Exchange(w, 8, rings, lambda n, b=a: wb.at[b, pl.ds(0, n)], p1[g - 3].k if g > 2 else None))
 
     stz[...] = jnp.zeros_like(stz)
+    sty[...] = jnp.zeros_like(sty)
     own.wait()
     count = len(partners) + jnp.where(home, 0, 1) + jnp.where(s < 15, 1, 0)
     pl.semaphore_wait(barrier, count)
@@ -423,7 +424,7 @@
 
             @pl.when(z == i)
             def _(i=i):
-                w.arrive(z_k, stz.at[pl.ds(0, i)], at(z + 1, y))
+                w.arrive(z_k, stz.at[pl.ds(0, i), pl.ds(0, 130)], at(z + 1, y))
 
     def chip_weight(b, xx):
         top, low = ([wb[b, xx, 2 * k + j] for j in range(2)] for k in range(2))
@@ -474,7 +475,7 @@
     project_all(1, finish_fi)
     local_states()
     for i in (2, 1, 3):
-        w.start(6, y_k, sty.at[y], sty.at[y], at(z, y + i))
+        w.start(6, y_k, sty.at[y, pl.ds(0, 130)], sty.at[y, pl.ds(0, 130)], at(z, y + i))
 
     p2[2].relay()
     p1[3].rest()
@@ -486,7 +487,7 @@
     take_halo()
     convolve(0, 1)
     conv_ring.start()
-    w.arrive(y_k, sty.at[pl.ds(0, 3)], at(z, y + 1))
+    w.arrive(y_k, sty.at[pl.ds(0, 3), pl.ds(0, 130)], at(z, y + 1))
     row_decay, row_state = jnp.ones((1, HEAD), F32), jnp.zeros((HEAD, HEAD), F32)
     my_decay, my_state = row_decay, row_state
     for i in range(4):
@@ -501,7 +502,7 @@
 
         @pl.when(z + i < 4)
         def _(i=i):
-            w.start(7, z_k, stz.at[z], stz.at[z], at(z + i, y))
+            w.start(7, z_k, stz.at[z, pl.ds(0, 130)], stz.at[z, pl.ds(0, 130)], at(z + i, y))
 
 
     p1[5].rest()
@@ -615,12 +616,12 @@
     def _():
         w.left(5, hsend, following)
 
-    w.left(6, sty.at[pl.ds(0, 3)], mate)
+    w.left(6, sty.at[pl.ds(0, 3), pl.ds(0, 130)], mate)
     for i in (1, 2, 3):
 
         @pl.when(z == 3 - i)
         def _(i=i):
-            w.left(7, stz.at[pl.ds(0, i)], mate)
+            w.left(7, stz.at[pl.ds(0, i), pl.ds(0, 130)], mate)
 
 
 def local(

time: 49.7 us -> 49.6 us (level)
  no operation moved by 1% of the time
where the time goes in v12:
time: 49.6 us; the launch traced here: 49.4 us
  Pallas kernels  48.7 us (98%)
  local copies, waits for them, and re-layouts  0.75 us (2%)
    pallas_call x1, Pallas kernels, local(): pl.pallas_call(kernel, out_shape=jax.ShapeDtypeStruct((T, 256), BF16), in...  48.7 us

profile of v12, /device:TPU:1, one launch (start us, length us, event | category | flops | bytes accessed | tf_op | source)
XLA Modules:
  0.0 49.4 jit_solution(2985988176526250970)
XLA Ops:
  0.0 48.7 %shard_map.181 = bf16[768,256]{1,0:T(8,128)(2,1)S(1)} custom-call(bf16[96,2048]{1,0:T(8,128)(2,1)} %tokens.1, f32[1,2048]{1,0:T(1,128)} %bitcast.5, bf16[128,128]{1,0:T(8,128)(2,1)} %w_f.1, bf16[128,128]{1,0:T(8,128)(2,1)} %w_i.1, bf16[128,128]{1,0:T(8,128)(2,1)} %w_q.1, bf16[128,128]{1,0:T(8,128)(2,1)} %w_o.1, bf16[128,128]{1,0:T(8,128)(2,1)} %w_v.1, ...), custom_call_target="tpu_custom_call" | custom-call | tf_op jit(solution)/shard_map/pallas_call | solution.py:648
  48.7 0.7 %copy.21 = bf16[768,256]{1,0:T(8,128)(2,1)} copy(bf16[768,256]{1,0:T(8,128)(2,1)S(1)} %shard_map.181) | data formatting | bytes 786432

commit v13 on v12

--- a/solution.py
+++ b/solution.py
@@ -475,7 +475,11 @@
     project_all(1, finish_fi)
     local_states()
     for i in (2, 1, 3):
-        w.start(6, y_k, sty.at[y, pl.ds(0, 130)], sty.at[y, pl.ds(0, 130)], at(z, y + i))
+
+        @pl.when((z < 3) | (y + i < 4))
+        def _(i=i):
+            w.start(6, y_k, sty.at[y, pl.ds(0, 130)], sty.at[y, pl.ds(0, 130)], at(z, y + i))
+
 
     p2[2].relay()
     p1[3].rest()
@@ -487,7 +491,12 @@
     take_halo()
     convolve(0, 1)
     conv_ring.start()
-    w.arrive(y_k, sty.at[pl.ds(0, 3), pl.ds(0, 130)], at(z, y + 1))
+    for i in (1, 2, 3):
+
+        @pl.when((z == 3) & (y == i) if i < 3 else (z < 3) | (y == 3))
+        def _(i=i):
+            w.arrive(y_k, sty.at[pl.ds(0, i), pl.ds(0, 130)], at(z, y + 1))
+
     row_decay, row_state = jnp.ones((1, HEAD), F32), jnp.zeros((HEAD, HEAD), F32)
     my_decay, my_state = row_decay, row_state
     for i in range(4):
@@ -616,7 +625,12 @@
     def _():
         w.left(5, hsend, following)
 
-    w.left(6, sty.at[pl.ds(0, 3), pl.ds(0, 130)], mate)
+    for i in (1, 2, 3):
+
+        @pl.when((z == 3) & (y == 3 - i) if i < 3 else (z < 3) | (y == 0))
+        def _(i=i):
+            w.left(6, sty.at[pl.ds(0, i), pl.ds(0, 130)], mate)
+
     for i in (1, 2, 3):
 
         @pl.when(z == 3 - i)

time: 49.6 us -> 50 us (level)
  no operation moved by 1% of the time
where the time goes in v13:
time: 50 us; the launch traced here: 49.8 us
  Pallas kernels  49.1 us (98%)
  local copies, waits for them, and re-layouts  0.75 us (2%)
    pallas_call x1, Pallas kernels, local(): pl.pallas_call(kernel, out_shape=jax.ShapeDtypeStruct((T, 256), BF16), in...  49.1 us

profile of v13, /device:TPU:1, one launch (start us, length us, event | category | flops | bytes accessed | tf_op | source)
XLA Modules:
  0.0 49.8 jit_solution(4026389444457960098)
XLA Ops:
  0.0 49.1 %shard_map.181 = bf16[768,256]{1,0:T(8,128)(2,1)S(1)} custom-call(bf16[96,2048]{1,0:T(8,128)(2,1)} %tokens.1, f32[1,2048]{1,0:T(1,128)} %bitcast.5, bf16[128,128]{1,0:T(8,128)(2,1)} %w_f.1, bf16[128,128]{1,0:T(8,128)(2,1)} %w_i.1, bf16[128,128]{1,0:T(8,128)(2,1)} %w_q.1, bf16[128,128]{1,0:T(8,128)(2,1)} %w_o.1, bf16[128,128]{1,0:T(8,128)(2,1)} %w_v.1, ...), custom_call_target="tpu_custom_call" | custom-call | tf_op jit(solution)/shard_map/pallas_call | solution.py:662
  49.1 0.7 %copy.21 = bf16[768,256]{1,0:T(8,128)(2,1)} copy(bf16[768,256]{1,0:T(8,128)(2,1)S(1)} %shard_map.181) | data formatting | bytes 786432
